TPU v7x, 32 devices: a whole 2x2x4 slice. The times are simulated.
32 devices in a mesh: sp: 4 (over y, x), dp: 8 (over z, core).
Axes of the slice: x: 2, y: 2, z: 4, core: 2. Of those that a mesh axis runs over, the one named last changes fastest.
Arguments:
- tokens: bfloat16 [8, 1024, 2048], P('dp', 'sp'), may hold values from -6 to 6
- key_weight: bfloat16 [2048, 2048], P('dp'), may hold values from -0.125 to 0.125
- queries: bfloat16 [8, 1024, 16, 128], P('dp', None, 'sp'), may hold values from -1.5 to 1.5
- values: bfloat16 [8, 1024, 16, 256], P('dp', None, 'sp'), may hold values from -1.5 to 1.5
- cotangent: bfloat16 [8, 1024, 4096], P('dp', 'sp'), may hold values from -6 to 6
- log_decay: float32 [16], replicated, may hold values from -0.034 to 0, as said below
Outputs:
- grad_tokens: bfloat16 [8, 1024, 2048], P('dp', 'sp')
- grad_queries: bfloat16 [8, 1024, 16, 128], P('dp', None, 'sp')
- grad_values: bfloat16 [8, 1024, 16, 256], P('dp', None, 'sp')
- grad_key_weight: float32 [2048, 2048], P('dp')
Inputs may be any that keep to these rules, and one draw needn't show every extreme that they name: `log_decay`: every entry is below zero.
All inputs are finite; a program needn't handle non-finite values.
Results may differ from a plain program's by a relative error of at most 0.0075.
Values may be sent and summed in bfloat16 or wider, within the bound.
A program may use at most 128 MiB of HBM per device.

v0:
```python
import functools

import jax
import jax.numpy as jnp
import numpy as np
from jax import lax
from jax.experimental import pallas as pl
from jax.experimental.pallas import tpu as pltpu
from jax.sharding import PartitionSpec as P

BLOCK = 128
CORES = 2
MESH = pl.DeviceIdType.MESH
F32 = jnp.float32
BF16 = jnp.bfloat16
VMEM_LIMIT = 60 * 1024 * 1024


def rotation_tables(seq_len, half):
    position = np.arange(seq_len, dtype=np.float32)
    frequency = (10000.0 ** (-np.arange(half, dtype=np.float32) / half)).astype(np.float32)
    angle = (position[:, None] * frequency[None, :]).astype(np.float32)
    cosine, sine = np.cos(angle), np.sin(angle)
    return (
        np.concatenate([cosine, cosine], axis=1).astype(np.float32),
        np.concatenate([-sine, sine], axis=1).astype(np.float32),
    )


def dot_nt(a, b):
    return lax.dot_general(a, b, (((1,), (1,)), ((), ())), preferred_element_type=F32)


def dot_tn(a, b):
    return lax.dot_general(a, b, (((0,), (0,)), ((), ())), preferred_element_type=F32)


def dot_nn(a, b):
    return lax.dot_general(a, b, (((1,), (0,)), ((), ())), preferred_element_type=F32)


def retention_kernel(
    decay_ref, q_ref, k_ref, v_ref, c_ref, cos_ref, sin_ref,
    gq_ref, gk_ref, gkt_ref, gv_ref, rq_ref, rk_ref, mix_ref,
):
    seq_len, key_width = q_ref.shape
    value_width = v_ref.shape[1]
    nblocks = seq_len // BLOCK
    half = key_width // 2
    factor = key_width ** (-0.5)
    decay = decay_ref[lax.axis_index("sp") * pl.num_programs(0) + pl.program_id(0)]
    row = lax.broadcasted_iota(jnp.int32, (BLOCK, BLOCK), 0).astype(F32)
    col = lax.broadcasted_iota(jnp.int32, (BLOCK, BLOCK), 1).astype(F32)
    within = jnp.where(row >= col, jnp.exp(jnp.maximum(row - col, 0.0) * decay), 0.0)
    inside = lax.broadcasted_iota(jnp.int32, (BLOCK, key_width), 0).astype(F32)
    rising = jnp.exp((inside + 1.0) * decay)
    falling = jnp.exp((BLOCK - 1.0 - inside) * decay)
    wide = lax.broadcasted_iota(jnp.int32, (BLOCK, value_width), 0).astype(F32)
    falling_wide = jnp.exp((BLOCK - 1.0 - wide) * decay)
    carry_decay = jnp.exp(jnp.full((key_width, value_width), BLOCK * 1.0, F32) * decay)
    zero = jnp.zeros((key_width, value_width), F32)

    def forward(n, entering):
        rows = pl.ds(pl.multiple_of(n * BLOCK, BLOCK), BLOCK)
        cosine, sine = cos_ref[rows, :], sin_ref[rows, :]
        q = q_ref[rows, :].astype(F32)
        k = k_ref[rows, :].astype(F32)
        rq = (q * cosine + pltpu.roll(q, half, 1) * sine).astype(BF16)
        rk = ((k * cosine + pltpu.roll(k, half, 1) * sine) * factor).astype(BF16)
        rq_ref[rows, :] = rq
        rk_ref[rows, :] = rk
        v, c = v_ref[rows, :], c_ref[rows, :]
        mixing = (dot_nt(c, v) * within).astype(BF16)
        mix_ref[rows, :] = mixing
        grad = dot_nn(mixing, rk) + rising * dot_nt(c, entering.astype(BF16))
        gq_ref[rows, :] = (grad * cosine - pltpu.roll(grad, half, 1) * sine).astype(BF16)
        decayed = (rk.astype(F32) * falling).astype(BF16)
        return entering * carry_decay + dot_tn(decayed, v)

    def backward(step, trailing):
        n = nblocks - 1 - step
        rows = pl.ds(pl.multiple_of(n * BLOCK, BLOCK), BLOCK)
        cosine, sine = cos_ref[rows, :], sin_ref[rows, :]
        rq, rk, mixing = rq_ref[rows, :], rk_ref[rows, :], mix_ref[rows, :]
        v, c = v_ref[rows, :], c_ref[rows, :]
        held = trailing.astype(BF16)
        scores = (dot_nt(rq, rk) * within).astype(BF16)
        grad = dot_tn(mixing, rq) + falling * dot_nt(v, held)
        back = (grad * cosine - pltpu.roll(grad, half, 1) * sine) * factor
        gk_ref[rows, :] = back.astype(BF16)
        gkt_ref[:, rows] = back.T.astype(BF16)
        gv_ref[rows, :] = (dot_tn(scores, c) + falling_wide * dot_nn(rk, held)).astype(BF16)
        decayed = (rq.astype(F32) * rising).astype(BF16)
        return trailing * carry_decay + dot_tn(decayed, c)

    unroll = min(nblocks, 8)
    lax.fori_loop(0, nblocks, forward, zero, unroll=unroll)
    lax.fori_loop(0, nblocks, backward, zero, unroll=unroll)


def retention_backward(queries, keys, values, cotan, decay, heads):
    seq_len = queries.shape[0]
    kw = queries.shape[1] // heads
    vw = values.shape[1] // heads
    cosine, sine = rotation_tables(seq_len, kw // 2)
    narrow = pl.BlockSpec((seq_len, kw), lambda h: (0, h))
    wide = pl.BlockSpec((seq_len, vw), lambda h: (0, h))
    table = pl.BlockSpec((seq_len, kw), lambda h: (0, 0))
    flops = 2 * seq_len * heads * BLOCK * (3 * kw + 2 * vw + 5 * vw)
    return pl.pallas_call(
        retention_kernel,
        grid=(heads,),
        in_specs=[pl.BlockSpec(memory_space=pltpu.SMEM), narrow, narrow, wide, wide, table, table],
        out_specs=[narrow, narrow, pl.BlockSpec((kw, seq_len), lambda h: (h, 0)), wide],
        out_shape=[
            jax.ShapeDtypeStruct(queries.shape, BF16),
            jax.ShapeDtypeStruct(queries.shape, BF16),
            jax.ShapeDtypeStruct(queries.shape[::-1], BF16),
            jax.ShapeDtypeStruct(values.shape, BF16),
        ],
        scratch_shapes=[
            pltpu.VMEM((seq_len, kw), BF16),
            pltpu.VMEM((seq_len, kw), BF16),
            pltpu.VMEM((seq_len, BLOCK), BF16),
        ],
        compiler_params=pltpu.CompilerParams(vmem_limit_bytes=VMEM_LIMIT),
        cost_estimate=pl.CostEstimate(
            flops=flops, bytes_accessed=8 * seq_len * heads * (kw + vw), transcendentals=0
        ),
        name="retention",
    )(decay, queries, keys, values, cotan, jnp.asarray(cosine), jnp.asarray(sine))


def remote(src, dst, send, recv, target):
    return pltpu.make_async_remote_copy(
        src_ref=src, dst_ref=dst, send_sem=send, recv_sem=recv,
        device_id=target, device_id_type=MESH,
    )


def greet(nsp, nz, s, z, core):
    barrier = pltpu.get_barrier_semaphore()
    others = [{"dp": z * CORES + 1 - core}]
    others += [{"sp": (s + j) % nsp} for j in range(1, nsp)]
    others += [{"dp": (z + j) % nz * CORES + core} for j in range(1, nz)]
    for other in others:
        pl.semaphore_signal(barrier, inc=1, device_id=other, device_id_type=MESH)
    pl.semaphore_wait(barrier, len(others))


CHUNKS = 4
TILE = 256


def gather_kernel(
    nsp, nz, tok, weight, cot, tall, wsel, call, keys,
    tok_send, tok_recv, cot_send, cot_recv, up_send, down_send, chain_recv, pair_send, pair_recv,
):
    s = lax.axis_index("sp")
    k = lax.axis_index("dp")
    z, core = k // CORES, k % CORES
    greet(nsp, nz, s, z, core)
    x, y = s % 2, s // 2
    xn, yn = y * 2 + (1 - x), (1 - y) * 2 + x
    rows, width = tok.shape
    wrows = weight.shape[0]
    cwidth = call.shape[1]
    piece = wrows // CHUNKS
    hrows = rows // 2

    def own_rows(ref, who):
        return ref.at[pl.ds(pl.multiple_of(who * rows, rows), rows), :]

    def half_rows(who, h):
        start = pl.multiple_of(who * rows + h * hrows, hrows)
        return tall.at[pl.ds(start, hrows), :]

    def token(i, src, who, h, target):
        return remote(src, half_rows(who, h), tok_send.at[i], tok_recv.at[i], {"sp": target})

    def own_half(h):
        return tok.at[pl.ds(h * hrows, hrows), :]

    diagonal = (1 - y) * 2 + (1 - x)
    sends = [
        token(0, own_half(0), s, 0, xn),
        token(1, own_half(1), s, 1, yn),
        token(2, own_half(1), s, 1, xn),
        token(3, own_half(0), s, 0, yn),
        token(4, half_rows(xn, 0), xn, 0, yn),
        token(5, half_rows(yn, 1), yn, 1, xn),
    ]
    arrivals = [
        token(0, own_half(0), xn, 0, xn),
        token(1, own_half(1), yn, 1, yn),
        token(2, own_half(1), xn, 1, xn),
        token(3, own_half(0), yn, 0, yn),
        token(4, own_half(0), diagonal, 0, yn),
        token(5, own_half(1), diagonal, 1, xn),
    ]
    for copy in sends[:4]:
        copy.start()

    def part(side, i):
        return wsel.at[pl.ds(pl.multiple_of(side * wrows + i * piece, piece), piece), :]

    up = {"dp": k + CORES}
    down = {"dp": k - CORES}
    partner = {"dp": z * CORES + 1 - core}
    owner = z == s

    @pl.when(owner)
    def _():
        wsel[pl.ds(pl.multiple_of(core * wrows, wrows), wrows), :] = weight[...]

    for i in range(CHUNKS):
        src = weight.at[pl.ds(i * piece, piece), :]

        @pl.when(owner & (z < nz - 1))
        def _():
            remote(src, part(core, i), up_send.at[i], chain_recv.at[i], up).start()

        @pl.when(owner & (z > 0))
        def _():
            remote(src, part(core, i), down_send.at[i], chain_recv.at[i], down).start()

        @pl.when(owner)
        def _():
            remote(src, part(core, i), pair_send.at[i], pair_recv.at[i], partner).start()

    tall[pl.ds(pl.multiple_of(s * rows, rows), rows), :] = tok[...]
    call[pl.ds(pl.multiple_of(s * rows, rows), rows), :] = cot[
        :, pl.ds(pl.multiple_of(s * cwidth, cwidth), cwidth)
    ]

    arrivals[0].wait_recv()
    sends[4].start()
    arrivals[1].wait_recv()
    sends[5].start()

    peers = []
    for j in range(1, nsp):
        peer = (s + j) % nsp
        source = (s - j + nsp) % nsp
        columns = pl.ds(pl.multiple_of(peer * cwidth, cwidth), cwidth)
        out_cot = remote(
            cot.at[:, columns], own_rows(call, s), cot_send.at[j], cot_recv.at[j], {"sp": peer}
        )
        in_cot = remote(
            cot.at[:, columns], own_rows(call, source), cot_send.at[j], cot_recv.at[j], {"sp": peer}
        )
        peers.append((out_cot, in_cot))
    for out_cot, _ in peers:
        out_cot.start()

    for i in range(CHUNKS):
        @pl.when(z != s)
        def _():
            remote(part(core, i), part(core, i), up_send.at[i], chain_recv.at[i], partner).wait_recv()

        @pl.when((z > s) & (z < nz - 1))
        def _():
            remote(part(core, i), part(core, i), up_send.at[i], chain_recv.at[i], up).start()

        @pl.when((z < s) & (z > 0))
        def _():
            remote(part(core, i), part(core, i), down_send.at[i], chain_recv.at[i], down).start()

        @pl.when(z != s)
        def _():
            remote(part(core, i), part(core, i), pair_send.at[i], pair_recv.at[i], partner).start()

    for i in range(CHUNKS):
        other = part(1 - core, i)
        remote(other, other, pair_send.at[i], pair_recv.at[i], partner).wait_recv()
    for arrive in arrivals[2:]:
        arrive.wait_recv()

    def project(i, _):
        at = pl.ds(pl.multiple_of(i * TILE, TILE), TILE)
        keys[at, :] = dot_nt(tall[at, :], wsel[...]).astype(BF16)
        return 0

    lax.fori_loop(0, tall.shape[0] // TILE, project, 0)

    for i in range(CHUNKS):
        mine = part(core, i)

        @pl.when((z >= s) & (z < nz - 1))
        def _():
            remote(mine, mine, up_send.at[i], chain_recv.at[i], up).wait_send()

        @pl.when((z <= s) & (z > 0))
        def _():
            remote(mine, mine, down_send.at[i], chain_recv.at[i], down).wait_send()

        remote(mine, mine, pair_send.at[i], pair_recv.at[i], partner).wait_send()
    for copy in sends:
        copy.wait_send()
    for out_cot, in_cot in peers:
        out_cot.wait_send()
        in_cot.wait_recv()


def gather(tokens, weight, cotan, nsp, ndp):
    rows, width = tokens.shape
    wrows = weight.shape[0]
    dma = pltpu.SemaphoreType.DMA
    vmem = pl.BlockSpec(memory_space=pltpu.VMEM)
    return pl.pallas_call(
        functools.partial(gather_kernel, nsp, ndp // CORES),
        in_specs=[vmem] * 3,
        out_specs=[vmem] * 4,
        out_shape=[
            jax.ShapeDtypeStruct((rows * nsp, width), BF16),
            jax.ShapeDtypeStruct((wrows * CORES, weight.shape[1]), BF16),
            jax.ShapeDtypeStruct((rows * nsp, cotan.shape[1] // nsp), BF16),
            jax.ShapeDtypeStruct((rows * nsp, wrows * CORES), BF16),
        ],
        scratch_shapes=[dma((6,))] * 2 + [dma((nsp,))] * 2 + [dma((CHUNKS,))] * 5,
        compiler_params=pltpu.CompilerParams(
            has_side_effects=True, vmem_limit_bytes=VMEM_LIMIT, collective_id=0
        ),
        name="gather",
    )(tokens, weight, cotan)


PARTS = 2


def scatter_kernel(
    nsp, nz, gk, gkt, tall, wsel, gt, gw,
    tsend, trecv, tmid, tlast, pwo, rp, zsum, rz, held, plane, final,
    t_send, t_recv, pair_send, pair_recv, z_send, z_recv,
    plane_send, plane_recv, final_send, final_recv,
):
    s = lax.axis_index("sp")
    k = lax.axis_index("dp")
    z, core = k // CORES, k % CORES
    greet(nsp, nz, s, z, core)
    x, y = s % 2, s // 2
    xn, yn = y * 2 + (1 - x), (1 - y) * 2 + x
    diagonal = (1 - y) * 2 + (1 - x)
    rows = gt.shape[0]
    half = gw.shape[0]
    width = gt.shape[1]
    cols = width // PARTS
    piece = half // nz
    partner = {"dp": z * CORES + 1 - core}
    step = 16

    def weight_part(side, c, out):
        left = pl.ds(pl.multiple_of(side * half, half), half)

        def tile(i, _):
            at = pl.ds(pl.multiple_of(c * cols + i * TILE, TILE), TILE)
            to = pl.ds(pl.multiple_of(i * TILE, TILE), TILE)
            out(to, dot_nn(gkt[left, :], tall[:, at]))
            return 0

        lax.fori_loop(0, cols // TILE, tile, 0)

    def token_part(who, c, out):
        left = pl.ds(pl.multiple_of(who * rows, rows), rows)

        def tile(i, _):
            at = pl.ds(pl.multiple_of(c * cols + i * TILE, TILE), TILE)
            to = pl.ds(pl.multiple_of(i * TILE, TILE), TILE)
            out(to, dot_nn(gk[left, :], wsel[:, at]))
            return 0

        lax.fori_loop(0, cols // TILE, tile, 0)

    first, second = (xn, yn), (yn, xn)

    hops = []
    for c in range(2):
        for slot in range(2):
            i = 2 * c + slot
            hops.append(
                remote(tsend.at[i], trecv.at[i], t_send.at[i], t_recv.at[i], {"sp": first[c]})
            )

    pairs = [
        remote(pwo.at[c], rp.at[c], pair_send.at[c], pair_recv.at[c], partner)
        for c in range(PARTS)
    ]

    def put_token(i):
        def out(to, value):
            tsend[i, :, to] = value.astype(BF16)
        return out

    def put_weight(c):
        def out(to, value):
            pwo[c, :, to] = value.astype(BF16)
        return out

    weight_part(1 - core, 0, put_weight(0))
    pairs[0].start()
    for c in range(2):
        token_part(diagonal, c, put_token(2 * c))
        hops[2 * c].start()
    weight_part(1 - core, 1, put_weight(1))
    pairs[1].start()

    along = []
    for c in range(PARTS):
        pairs[c].wait_recv()

        def put_sum(to, value):
            zsum[c, :, to] = (value + rp[c, :, to].astype(F32)).astype(BF16)

        weight_part(core, c, put_sum)
        row = []
        for j in range(1, nz):
            to = (z + j) % nz
            i = c * nz + j
            row.append(
                remote(
                    zsum.at[c, pl.ds(pl.multiple_of(to * piece, piece), piece), :],
                    rz.at[c, j - 1], z_send.at[i], z_recv.at[i], {"dp": to * CORES + core},
                )
            )
        for copy in row:
            copy.start()
        along.append(row)
        token_part(first[c], c, put_token(2 * c + 1))
        hops[2 * c + 1].start()

    inplane = []
    for c in range(PARTS):
        for copy in along[c]:
            copy.wait_recv()

        def add_z(i, _):
            at = pl.ds(pl.multiple_of(i * step, step), step)
            mine = pl.ds(pl.multiple_of(z * piece + i * step, step), step)
            total = zsum[c, mine, :].astype(F32)
            for j in range(nz - 1):
                total = total + rz[c, j, at, :].astype(F32)
            held[c, at, :] = total.astype(BF16)
            return 0

        lax.fori_loop(0, piece // step, add_z, 0)
        row = []
        for j in range(1, nsp):
            peer = (s + j) % nsp
            source = (s - j + nsp) % nsp
            i = c * nsp + j
            row.append(
                (
                    remote(
                        held.at[c], plane.at[c, s],
                        plane_send.at[i], plane_recv.at[i], {"sp": peer},
                    ),
                    remote(
                        held.at[c], plane.at[c, source],
                        plane_send.at[i], plane_recv.at[i], {"sp": peer},
                    ),
                )
            )
        for out, _ in row:
            out.start()
        plane[c, s] = held[c]
        inplane.append(row)

    seconds = []
    for c in range(2):
        hops[2 * c].wait_recv()

        def put_mid(to, value):
            tmid[c, :, to] = (value + trecv[2 * c, :, to].astype(F32)).astype(BF16)

        token_part(second[c], c, put_mid)
        copy = remote(
            tmid.at[c], tlast.at[c], t_send.at[4 + c], t_recv.at[4 + c], {"sp": second[c]}
        )
        copy.start()
        seconds.append(copy)

    last = []
    for c in range(PARTS):
        for _, arrive in inplane[c]:
            arrive.wait_recv()
        for j in range(1, nz):
            to = (z + j) % nz
            source = (z - j + nz) % nz
            target = {"dp": to * CORES + core}
            i = c * nz + j
            pairing = (
                remote(
                    plane.at[c, to], final.at[c, z], final_send.at[i], final_recv.at[i], target
                ),
                remote(
                    plane.at[c, to], final.at[c, source],
                    final_send.at[i], final_recv.at[i], target,
                ),
            )
            pairing[0].start()
            last.append(pairing)
        final[c, z] = plane[c, z]

    for c in range(2):
        hops[2 * c + 1].wait_recv()
        seconds[c].wait_recv()
        left = pl.ds(pl.multiple_of(s * rows, rows), rows)
        for i in range(cols // TILE):
            at = pl.ds(c * cols + i * TILE, TILE)
            to = pl.ds(i * TILE, TILE)
            value = dot_nn(gk[left, :], wsel[:, at])
            value = value + trecv[2 * c + 1, :, to].astype(F32)
            gt[:, at] = (value + tlast[c, :, to].astype(F32)).astype(BF16)

    for copy in hops + seconds + pairs:
        copy.wait_send()
    for row in along:
        for copy in row:
            copy.wait_send()
    for row in inplane:
        for out, _ in row:
            out.wait_send()
    for out, arrive in last:
        out.wait_send()
        arrive.wait_recv()
    for c in range(PARTS):
        for p in range(nz):
            def widen(i, _):
                to = pl.ds(pl.multiple_of(p * piece + i * step, step), step)
                at = pl.ds(pl.multiple_of(i * step, step), step)
                gw[to, pl.ds(c * cols, cols)] = final[c, p, at, :].astype(F32)
                return 0

            lax.fori_loop(0, piece // step, widen, 0)


def scatter(grad_key, grad_key_t, all_tokens, weight, nsp, ndp):
    nz = ndp // CORES
    rows, width = all_tokens.shape[0] // nsp, all_tokens.shape[1]
    half = grad_key.shape[1] // CORES
    cols = width // PARTS
    piece = half // nz
    dma = pltpu.SemaphoreType.DMA
    vmem = pl.BlockSpec(memory_space=pltpu.VMEM)
    return pl.pallas_call(
        functools.partial(scatter_kernel, nsp, nz),
        in_specs=[vmem] * 4,
        out_specs=[vmem] * 2,
        out_shape=[
            jax.ShapeDtypeStruct((rows, width), BF16),
            jax.ShapeDtypeStruct((half, width), F32),
        ],
        scratch_shapes=[
            pltpu.VMEM((4, rows, cols), BF16),
            pltpu.VMEM((4, rows, cols), BF16),
            pltpu.VMEM((2, rows, cols), BF16),
            pltpu.VMEM((2, rows, cols), BF16),
            pltpu.VMEM((PARTS, half, cols), BF16),
            pltpu.VMEM((PARTS, half, cols), BF16),
            pltpu.VMEM((PARTS, half, cols), BF16),
            pltpu.VMEM((PARTS, nz - 1, piece, cols), BF16),
            pltpu.VMEM((PARTS, piece, cols), BF16),
            pltpu.VMEM((PARTS, nsp, piece, cols), BF16),
            pltpu.VMEM((PARTS, nz, piece, cols), BF16),
            dma((6,)), dma((6,)), dma((PARTS,)), dma((PARTS,)),
            dma((PARTS * nz,)), dma((PARTS * nz,)),
            dma((PARTS * nsp,)), dma((PARTS * nsp,)),
            dma((PARTS * nz,)), dma((PARTS * nz,)),
        ],
        compiler_params=pltpu.CompilerParams(
            has_side_effects=True, vmem_limit_bytes=VMEM_LIMIT, collective_id=1
        ),
        name="scatter",
    )(grad_key, grad_key_t, all_tokens, weight)


def gather_general(tokens, weight, cotan):
    gathered = lax.all_gather(weight, "dp", axis=0, tiled=True)
    rows = gathered.shape[0] // lax.axis_size("sp")
    chosen = lax.dynamic_slice_in_dim(gathered, lax.axis_index("sp") * rows, rows)
    return (
        lax.all_gather(tokens, "sp", axis=0, tiled=True),
        chosen,
        lax.all_to_all(cotan, "sp", split_axis=1, concat_axis=0, tiled=True),
    )


def scatter_general(partial_tokens, partial_weight):
    grad_tokens = lax.psum_scatter(
        partial_tokens, "sp", scatter_dimension=0, tiled=True
    ).astype(BF16)
    owned = lax.psum_scatter(
        partial_weight, "dp", scatter_dimension=0, tiled=True
    )
    everything = lax.all_gather(owned, ("sp", "dp"), axis=0, tiled=True)
    rows = everything.shape[0] // lax.axis_size("dp")
    return grad_tokens, lax.dynamic_slice_in_dim(
        everything, lax.axis_index("dp") * rows, rows
    )


def body(nsp, ndp, tokens, key_weight, queries, values, cotangent, log_decay):
    direct = nsp == 4 and ndp == CORES * nsp
    heads = queries.shape[2]
    if direct:
        all_tokens, weight, cotan, keys = gather(tokens[0], key_weight, cotangent[0], nsp, ndp)
    else:
        all_tokens, weight, cotan = gather_general(tokens[0], key_weight, cotangent[0])
        keys = dot_nt(all_tokens, weight).astype(BF16)
    seq_len = all_tokens.shape[0]
    grad_query, grad_key, grad_key_t, grad_value = retention_backward(
        queries.reshape(seq_len, -1), keys, values.reshape(seq_len, -1), cotan, log_decay, heads
    )
    if direct:
        grad_tokens, weight_grad = scatter(
            grad_key, grad_key_t, all_tokens, weight, nsp, ndp
        )
    else:
        grad_tokens, weight_grad = scatter_general(
            dot_nn(grad_key, weight), dot_tn(grad_key, all_tokens)
        )
    return (
        grad_tokens[None],
        grad_query.reshape(queries.shape),
        grad_value.reshape(values.shape),
        weight_grad,
    )


def solution(mesh):
    return jax.shard_map(
        functools.partial(body, mesh.shape["sp"], mesh.shape["dp"]),
        mesh=mesh,
        in_specs=(
            P("dp", "sp", None),
            P("dp", None),
            P("dp", None, "sp", None),
            P("dp", None, "sp", None),
            P("dp", "sp", None),
            P(),
        ),
        out_specs=(
            P("dp", "sp", None),
            P("dp", None, "sp", None),
            P("dp", None, "sp", None),
            P("dp", None),
        ),
        check_vma=False,
    )
```

profile of v0, /device:TPU:0, one launch (start us, length us, event | category | flops | bytes accessed | tf_op | source)
XLA Modules:
  0.0 160.5 jit_solution(9011208601527353395)
XLA Ops:
  0.6 0.0 copy-start
  0.6 2.5 %copy.15 = bf16[128,8,4,128]{3,1,2,0:T(8,128)(2,1)} copy(bf16[128,8,4,128]{3,2,1,0:T(4,128)(2,1)} %bitcast.14) | data formatting | bytes 2097152
  3.2 0.0 copy-done
  3.2 1.8 %copy.13 = bf16[128,8,4,256]{3,1,2,0:T(8,128)(2,1)} copy(bf16[128,8,4,256]{3,2,1,0:T(4,128)(2,1)S(1)} %bitcast.11) | data formatting | bytes 4194304
  5.0 69.4 %gather.1 = (bf16[1024,2048]{1,0:T(8,128)(2,1)}, bf16[512,2048]{1,0:T(8,128)(2,1)}, bf16[1024,1024]{1,0:T(8,128)(2,1)}, bf16[1024,512]{1,0:T(8,128)(2,1)}) custom-call(bf16[256,2048]{1,0:T(8,128)(2,1)} %bitcast.17, bf16[256,2048]{1,0:T(8,128)(2,1)} %weight.1, bf16[256,4096]{1,0:T(8,128)(2,1)} %bitcast.12), custom_call_target="tpu_custom_call" | custom-call | tf_op jit(solution)/shard_map/gather/pallas_call | solution.py:310
  74.4 16.7 %retention.1 = (bf16[1024,512]{1,0:T(8,128)(2,1)}, bf16[1024,512]{1,0:T(8,128)(2,1)}, bf16[512,1024]{1,0:T(8,128)(2,1)}, bf16[1024,1024]{1,0:T(8,128)(2,1)}) custom-call(f32[16]{0:T(128)} %decay_ref.1, bf16[1024,512]{1,0:T(8,128)(2,1)} %bitcast.15, bf16[1024,512]{1,0:T(8,128)(2,1)} %get-tuple-element.14.k_ref, bf16[1024,1024]{1,0:T(8,128)(2,1)} %bitcast.13, ...), custom_call_target="tpu_custom_call" | custom-call | flops 2281701376 | bytes 12582912 | tf_op jit(solution)/shard_map/retention/pallas_call | solution.py:110
  91.1 0.0 copy-start.3
  91.2 61.4 %scatter.1 = (bf16[256,2048]{1,0:T(8,128)(2,1)}, f32[256,2048]{1,0:T(8,128)}) custom-call(bf16[1024,512]{1,0:T(8,128)(2,1)} %get-tuple-element.16.gk, bf16[512,1024]{1,0:T(8,128)(2,1)} %get-tuple-element.17.gkt, bf16[1024,2048]{1,0:T(8,128)(2,1)} %get-tuple-element.18.tall, bf16[512,2048]{1,0:T(8,128)(2,1)} %get-tuple-element.19.wsel), custom_call_target="tpu_custom_call" | custom-call | tf_op jit(solution)/shard_map/scatter/pallas_call | solution.py:545
  152.5 0.0 copy-start.1
  152.5 0.0 copy-done.3
  152.5 1.1 reshape.22
  153.7 0.8 copy-done.1
  154.5 0.0 copy-start.4
  154.5 2.7 %reshape.23 = bf16[1,1024,4,256]{3,2,1,0:T(4,128)(2,1)} reshape(bf16[1024,1024]{1,0:T(8,128)(2,1)S(1)} %copy-done.1) | data formatting | bytes 4194304 | tf_op jit(solution)/shard_map/reshape | solution.py:625
  157.2 0.0 copy-done.4
  157.2 0.0 copy-start.2
  157.2 1.0 copy.18
  158.2 1.0 copy-done.2
  159.2 1.3 copy.19
Async XLA Ops:
  0.6 2.5 %copy-start = (bf16[1,1024,4,256]{3,2,1,0:T(4,128)(2,1)S(1)}, bf16[1,1024,4,256]{3,2,1,0:T(4,128)(2,1)}, u32[]{:S(2)}) copy-start(bf16[1,1024,4,256]{3,2,1,0:T(4,128)(2,1)} %param.11) | copy-start | bytes 6291460
  91.1 61.4 %copy-start.3 = (bf16[1024,512]{1,0:T(8,128)(2,1)S(1)}, bf16[1024,512]{1,0:T(8,128)(2,1)}, u32[]{:S(2)}) copy-start(bf16[1024,512]{1,0:T(8,128)(2,1)} %get-tuple-element.21) | copy-start | bytes 3145732
  152.5 2.0 %copy-start.1 = (bf16[1024,1024]{1,0:T(8,128)(2,1)S(1)}, bf16[1024,1024]{1,0:T(8,128)(2,1)}, u32[]{:S(2)}) copy-start(bf16[1024,1024]{1,0:T(8,128)(2,1)} %get-tuple-element.22) | copy-start | bytes 6291460
  154.5 2.7 %copy-start.4 = (bf16[256,2048]{1,0:T(8,128)(2,1)S(1)}, bf16[256,2048]{1,0:T(8,128)(2,1)}, u32[]{:S(2)}) copy-start(bf16[256,2048]{1,0:T(8,128)(2,1)} %get-tuple-element.20) | copy-start | bytes 3145732
  157.2 2.0 %copy-start.2 = (f32[256,2048]{1,0:T(8,128)S(1)}, f32[256,2048]{1,0:T(8,128)}, u32[]{:S(2)}) copy-start(f32[256,2048]{1,0:T(8,128)} %get-tuple-element.31) | copy-start | bytes 6291460
where the time goes:
time: 161 us
  Pallas kernels  148 us (92%)
  local copies, waits for them, and re-layouts  12.3 us (8%)
    pallas_call x1, Pallas kernels, gather(): pl.pallas_call(functools.partial(gather_kernel, nsp, ndp // CORES), in_sp...  69.4 us
    pallas_call x1, Pallas kernels, scatter(): pl.pallas_call(functools.partial(scatter_kernel, nsp, nz), in_specs=[vmem...  61.4 us
    pallas_call x1, Pallas kernels, retention_backward(): pl.pallas_call(retention_kernel, grid=(heads,), in_specs=[pl.BlockSpec(me...  16.7 us
    unnamed x14, local copies, waits for them, and re-layouts  8.49 us

commit v1 on v0

v1 whole, which is shorter than its diff:
```python
import functools

import jax
import jax.numpy as jnp
import numpy as np
from jax import lax
from jax.experimental import pallas as pl
from jax.experimental.pallas import tpu as pltpu
from jax.sharding import PartitionSpec as P

BLOCK = 128
CORES = 2
MESH = pl.DeviceIdType.MESH
F32 = jnp.float32
BF16 = jnp.bfloat16
VMEM_LIMIT = 60 * 1024 * 1024


def rotation_tables(seq_len, half):
    position = np.arange(seq_len, dtype=np.float32)
    frequency = (10000.0 ** (-np.arange(half, dtype=np.float32) / half)).astype(np.float32)
    angle = (position[:, None] * frequency[None, :]).astype(np.float32)
    cosine, sine = np.cos(angle), np.sin(angle)
    return (
        np.concatenate([cosine, cosine], axis=1).astype(np.float32),
        np.concatenate([-sine, sine], axis=1).astype(np.float32),
    )


def dot_nt(a, b):
    return lax.dot_general(a, b, (((1,), (1,)), ((), ())), preferred_element_type=F32)


def dot_tn(a, b):
    return lax.dot_general(a, b, (((0,), (0,)), ((), ())), preferred_element_type=F32)


def dot_nn(a, b):
    return lax.dot_general(a, b, (((1,), (0,)), ((), ())), preferred_element_type=F32)


def retention_kernel(
    decay_ref, q_ref, k_ref, v_ref, c_ref, cos_ref, sin_ref,
    gq_ref, gk_ref, gkt_ref, gv_ref, rq_ref, rk_ref, mix_ref,
):
    seq_len, key_width = q_ref.shape
    value_width = v_ref.shape[1]
    nblocks = seq_len // BLOCK
    half = key_width // 2
    factor = key_width ** (-0.5)
    decay = decay_ref[lax.axis_index("sp") * pl.num_programs(0) + pl.program_id(0)]
    row = lax.broadcasted_iota(jnp.int32, (BLOCK, BLOCK), 0).astype(F32)
    col = lax.broadcasted_iota(jnp.int32, (BLOCK, BLOCK), 1).astype(F32)
    within = jnp.where(row >= col, jnp.exp(jnp.maximum(row - col, 0.0) * decay), 0.0)
    inside = lax.broadcasted_iota(jnp.int32, (BLOCK, key_width), 0).astype(F32)
    rising = jnp.exp((inside + 1.0) * decay)
    falling = jnp.exp((BLOCK - 1.0 - inside) * decay)
    wide = lax.broadcasted_iota(jnp.int32, (BLOCK, value_width), 0).astype(F32)
    falling_wide = jnp.exp((BLOCK - 1.0 - wide) * decay)
    carry_decay = jnp.exp(jnp.full((key_width, value_width), BLOCK * 1.0, F32) * decay)
    zero = jnp.zeros((key_width, value_width), F32)

    def forward(n, entering):
        rows = pl.ds(pl.multiple_of(n * BLOCK, BLOCK), BLOCK)
        cosine, sine = cos_ref[rows, :], sin_ref[rows, :]
        q = q_ref[rows, :].astype(F32)
        k = k_ref[rows, :].astype(F32)
        rq = (q * cosine + pltpu.roll(q, half, 1) * sine).astype(BF16)
        rk = ((k * cosine + pltpu.roll(k, half, 1) * sine) * factor).astype(BF16)
        rq_ref[rows, :] = rq
        rk_ref[rows, :] = rk
        v, c = v_ref[rows, :], c_ref[rows, :]
        mixing = (dot_nt(c, v) * within).astype(BF16)
        mix_ref[rows, :] = mixing
        grad = dot_nn(mixing, rk) + rising * dot_nt(c, entering.astype(BF16))
        gq_ref[rows, :] = (grad * cosine - pltpu.roll(grad, half, 1) * sine).astype(BF16)
        decayed = (rk.astype(F32) * falling).astype(BF16)
        return entering * carry_decay + dot_tn(decayed, v)

    def backward(step, trailing):
        n = nblocks - 1 - step
        rows = pl.ds(pl.multiple_of(n * BLOCK, BLOCK), BLOCK)
        cosine, sine = cos_ref[rows, :], sin_ref[rows, :]
        rq, rk, mixing = rq_ref[rows, :], rk_ref[rows, :], mix_ref[rows, :]
        v, c = v_ref[rows, :], c_ref[rows, :]
        held = trailing.astype(BF16)
        scores = (dot_nt(rq, rk) * within).astype(BF16)
        grad = dot_tn(mixing, rq) + falling * dot_nt(v, held)
        back = (grad * cosine - pltpu.roll(grad, half, 1) * sine) * factor
        gk_ref[rows, :] = back.astype(BF16)
        gkt_ref[:, rows] = back.T.astype(BF16)
        gv_ref[rows, :] = (dot_tn(scores, c) + falling_wide * dot_nn(rk, held)).astype(BF16)
        decayed = (rq.astype(F32) * rising).astype(BF16)
        return trailing * carry_decay + dot_tn(decayed, c)

    unroll = min(nblocks, 8)
    lax.fori_loop(0, nblocks, forward, zero, unroll=unroll)
    lax.fori_loop(0, nblocks, backward, zero, unroll=unroll)


def retention_backward(queries, keys, values, cotan, decay, heads):
    seq_len = queries.shape[0]
    kw = queries.shape[1] // heads
    vw = values.shape[1] // heads
    cosine, sine = rotation_tables(seq_len, kw // 2)
    narrow = pl.BlockSpec((seq_len, kw), lambda h: (0, h))
    wide = pl.BlockSpec((seq_len, vw), lambda h: (0, h))
    table = pl.BlockSpec((seq_len, kw), lambda h: (0, 0))
    flops = 2 * seq_len * heads * BLOCK * (3 * kw + 2 * vw + 5 * vw)
    return pl.pallas_call(
        retention_kernel,
        grid=(heads,),
        in_specs=[pl.BlockSpec(memory_space=pltpu.SMEM), narrow, narrow, wide, wide, table, table],
        out_specs=[narrow, narrow, pl.BlockSpec((kw, seq_len), lambda h: (h, 0)), wide],
        out_shape=[
            jax.ShapeDtypeStruct(queries.shape, BF16),
            jax.ShapeDtypeStruct(queries.shape, BF16),
            jax.ShapeDtypeStruct(queries.shape[::-1], BF16),
            jax.ShapeDtypeStruct(values.shape, BF16),
        ],
        scratch_shapes=[
            pltpu.VMEM((seq_len, kw), BF16),
            pltpu.VMEM((seq_len, kw), BF16),
            pltpu.VMEM((seq_len, BLOCK), BF16),
        ],
        compiler_params=pltpu.CompilerParams(vmem_limit_bytes=VMEM_LIMIT),
        cost_estimate=pl.CostEstimate(
            flops=flops, bytes_accessed=8 * seq_len * heads * (kw + vw), transcendentals=0
        ),
        name="retention",
    )(decay, queries, keys, values, cotan, jnp.asarray(cosine), jnp.asarray(sine))


def remote(src, dst, send, recv, target):
    return pltpu.make_async_remote_copy(
        src_ref=src, dst_ref=dst, send_sem=send, recv_sem=recv,
        device_id=target, device_id_type=MESH,
    )


def greet(nsp, nz, s, z, core):
    barrier = pltpu.get_barrier_semaphore()
    others = [{"dp": z * CORES + 1 - core}]
    others += [{"sp": (s + j) % nsp} for j in range(1, nsp)]
    others += [{"dp": (z + j) % nz * CORES + core} for j in range(1, nz)]
    for other in others:
        pl.semaphore_signal(barrier, inc=1, device_id=other, device_id_type=MESH)
    pl.semaphore_wait(barrier, len(others))


TILE = 256
LANES = 128
COLS = 256


def whole_kernel(
    nsp, nz, heads,
    decay_ref, tok_in, w_in, q_in, v_in, cot_in, cos_in, sin_in,
    gt_out, gq_out, gv_out, gw_out,
    cotv, tall, wall, call, q4, v8, cosv, sinv, rq, vals, mix, held, gk, gkt, gkall,
    keys, gq4, gv8, gt, acc, pwo, rp, lrecv, lsend, fin, xs, ys,
    within, rising, falling, carry, entering,
    load, cot_send, cot_recv, tok_send, tok_recv,
    up_send, up_recv, down_send, down_recv, pair_send, pair_recv,
    gk_send, gk_recv, half_send, half_recv, line_send, line_recv,
    cast_send, cast_recv, gq_store, gv_store, gw_store, gt_store,
):
    s = lax.axis_index("sp")
    k = lax.axis_index("dp")
    z, core = k // CORES, k % CORES
    x, y = s % 2, s // 2
    xn, yn = y * 2 + (1 - x), (1 - y) * 2 + x
    diagonal = (1 - y) * 2 + (1 - x)
    partner = {"dp": z * CORES + 1 - core}
    up, down = {"dp": k + CORES}, {"dp": k - CORES}
    rows, width = tok_in.shape
    wrows = w_in.shape[0]
    seq_len, feats = gk.shape
    kw = feats // heads
    cwidth = call.shape[1]
    vw = cwidth // heads
    parts = vw // LANES
    nblocks = seq_len // BLOCK
    half = kw // 2
    factor = kw ** (-0.5)
    hrows = rows // 2
    nchunks = width // COLS
    pieces = heads
    prow = wrows // pieces

    loads = [
        pltpu.make_async_copy(cot_in, cotv, load.at[0]),
        pltpu.make_async_copy(w_in, wall.at[pl.ds(pl.multiple_of(k * wrows, wrows), wrows), :], load.at[1]),
        pltpu.make_async_copy(tok_in, tall.at[pl.ds(pl.multiple_of(s * rows, rows), rows), :], load.at[2]),
        pltpu.make_async_copy(
            cot_in.at[:, pl.ds(pl.multiple_of(s * cwidth, cwidth), cwidth)],
            call.at[pl.ds(pl.multiple_of(s * rows, rows), rows), :], load.at[3],
        ),
        pltpu.make_async_copy(q_in, q4, load.at[4]),
        pltpu.make_async_copy(v_in, v8, load.at[5]),
        pltpu.make_async_copy(cos_in, cosv, load.at[6]),
        pltpu.make_async_copy(sin_in, sinv, load.at[7]),
    ]
    for copy in loads:
        copy.start()
    greet(nsp, nz, s, z, core)

    def cot_copy(j, h, source):
        peer = (s + j) % nsp
        columns = pl.ds(pl.multiple_of(peer * cwidth + h * vw, vw), vw)
        to = call.at[
            pl.ds(pl.multiple_of(source * rows, rows), rows), pl.ds(pl.multiple_of(h * vw, vw), vw)
        ]
        i = j * heads + h
        return remote(cotv.at[:, columns], to, cot_send.at[i], cot_recv.at[i], {"sp": peer})

    loads[0].wait()
    for h in range(heads):
        for j in range(1, nsp):
            cot_copy(j, h, s).start()

    def piece(zb, c, p):
        start = pl.multiple_of((zb * CORES + c) * wrows + p * prow, prow)
        return wall.at[pl.ds(start, prow), :]

    def up_copy(d, p):
        ref, i = piece(z - d, core, p), d * pieces + p
        return remote(ref, ref, up_send.at[i], up_recv.at[i], up)

    def down_copy(d, p):
        ref, i = piece(z + d, core, p), d * pieces + p
        return remote(ref, ref, down_send.at[i], down_recv.at[i], down)

    def up_arrival(d, p):
        ref, i = piece(z - d, core, p), (d - 1) * pieces + p
        return remote(ref, ref, up_send.at[i], up_recv.at[i], partner)

    def down_arrival(d, p):
        ref, i = piece(z + d, core, p), (d - 1) * pieces + p
        return remote(ref, ref, down_send.at[i], down_recv.at[i], partner)

    def pair_copy(zb, p):
        ref, i = piece(zb, core, p), zb * pieces + p
        return remote(ref, ref, pair_send.at[i], pair_recv.at[i], partner)

    def pair_arrival(zb, p):
        ref, i = piece(zb, 1 - core, p), zb * pieces + p
        return remote(ref, ref, pair_send.at[i], pair_recv.at[i], partner)

    loads[1].wait()
    for p in range(pieces):
        @pl.when(z < nz - 1)
        def _():
            up_copy(0, p).start()

        @pl.when(z > 0)
        def _():
            down_copy(0, p).start()

        pair_copy(z, p).start()

    def relay(d, p):
        @pl.when(z >= d)
        def _():
            up_arrival(d, p).wait_recv()
            if d < nz - 1:
                @pl.when(z < nz - 1)
                def _():
                    up_copy(d, p).start()
            pair_copy(z - d, p).start()

        @pl.when(z + d < nz)
        def _():
            down_arrival(d, p).wait_recv()
            if d < nz - 1:
                @pl.when(z > 0)
                def _():
                    down_copy(d, p).start()
            pair_copy(z + d, p).start()

    def token(j, i, who, h, target):
        at = tall.at[
            pl.ds(pl.multiple_of(who * rows + h * hrows, hrows), hrows),
            pl.ds(pl.multiple_of(j * COLS, COLS), COLS),
        ]
        n = j * 6 + i
        return remote(at, at, tok_send.at[n], tok_recv.at[n], {"sp": target})

    def token_send(j, i):
        who, h, target = [
            (s, 0, xn), (s, 1, yn), (s, 1, xn), (s, 0, yn), (xn, 0, yn), (yn, 1, xn)
        ][i]
        return token(j, i, who, h, target)

    def token_arrival(j, i):
        who, h, target = [
            (xn, 0, xn), (yn, 1, yn), (xn, 1, xn), (yn, 0, yn), (diagonal, 0, yn), (diagonal, 1, xn)
        ][i]
        return token(j, i, who, h, target)

    loads[2].wait()
    for i in range(4):
        token_send(0, i).start()
    for copy in loads[3:]:
        copy.wait()

    def prepare(n, _):
        at = pl.ds(pl.multiple_of(n * BLOCK, BLOCK), BLOCK)
        cosine, sine = cosv[at, :], sinv[at, :]
        span = BLOCK * heads
        xs[...] = q4[pl.ds(pl.multiple_of(n * span, span), span), :].astype(F32)
        for h in range(heads):
            q = xs[pl.ds(h, BLOCK, stride=heads), :]
            rq[at, h * kw:(h + 1) * kw] = (q * cosine + pltpu.roll(q, half, 1) * sine).astype(BF16)
        span = BLOCK * heads * parts
        ys[...] = v8[pl.ds(pl.multiple_of(n * span, span), span), :].astype(F32)
        for h in range(heads):
            for i in range(parts):
                left = h * vw + i * LANES
                vals[at, left:left + LANES] = ys[
                    pl.ds(i * heads + h, BLOCK, stride=heads * parts), :
                ].astype(BF16)
        return 0

    lax.fori_loop(0, nblocks, prepare, 0)

    def key_head(h, _):
        relay(1, h)
        for j in range(1, nsp):
            cot_copy(j, h, (s - j + nsp) % nsp).wait_recv()
        kc = pl.ds(pl.multiple_of(h * kw, kw), kw)
        vc = pl.ds(pl.multiple_of(h * vw, vw), vw)
        decay = decay_ref[s * heads + h]
        row = lax.broadcasted_iota(jnp.int32, (BLOCK, BLOCK), 0).astype(F32)
        col = lax.broadcasted_iota(jnp.int32, (BLOCK, BLOCK), 1).astype(F32)
        inside = lax.broadcasted_iota(jnp.int32, (BLOCK, kw), 0).astype(F32)
        mask = jnp.where(row >= col, jnp.exp(jnp.maximum(row - col, 0.0) * decay), 0.0)
        rise = jnp.exp((inside + 1.0) * decay)
        fall = jnp.exp((BLOCK - 1.0 - inside) * decay)
        step = jnp.exp(jnp.full((8, vw), BLOCK * 1.0, F32) * decay)
        within[h] = mask
        rising[h] = rise
        falling[h] = fall
        carry[h] = step
        trailing = jnp.zeros((kw, vw), F32)
        for n in reversed(range(nblocks)):
            at = slice(n * BLOCK, (n + 1) * BLOCK)
            cosine, sine = cosv[at, :], sinv[at, :]
            q, v, c = rq[at, kc], vals[at, vc], call[at, vc]
            mixing = (dot_nt(c, v) * mask).astype(BF16)
            mix[at, pl.ds(pl.multiple_of(h * BLOCK, BLOCK), BLOCK)] = mixing
            trail = trailing.astype(BF16)
            held[h * nblocks + n] = trail
            grad = dot_tn(mixing, q) + fall * dot_nt(v, trail)
            back = (grad * cosine - pltpu.roll(grad, half, 1) * sine) * factor
            gk[at, kc] = back.astype(BF16)
            gkt[kc, at] = back.T.astype(BF16)
            decayed = (q.astype(F32) * rise).astype(BF16)
            trailing = trailing * step[0:1, :] + dot_tn(decayed, c)
        entering[h] = jnp.zeros((kw, vw), F32)
        return 0

    lax.fori_loop(0, heads, key_head, 0)

    def gk_copy(j, source):
        peer = (s + j) % nsp
        to = gkall.at[:, pl.ds(pl.multiple_of(source * feats, feats), feats)]
        return remote(
            gk.at[pl.ds(pl.multiple_of(peer * rows, rows), rows), :], to,
            gk_send.at[j], gk_recv.at[j], {"sp": peer},
        )

    def half_copy(j):
        return remote(pwo.at[j], rp.at[j], half_send.at[j], half_recv.at[j], partner)

    def line_copy(j, side, target):
        return remote(
            lsend.at[j], lrecv.at[side, j], line_send.at[j],
            line_recv.at[side * nchunks + j], target,
        )

    def cast_copy(j, h, target):
        ref = fin.at[j, pl.ds(h * (wrows // 2), wrows // 2), :]
        i = 2 * j + h
        return remote(ref, ref, cast_send.at[i], cast_recv.at[i], {"sp": target})

    far = jnp.maximum(z, nz - 1 - z)
    behind = jnp.where(z > s, nz - 1 - z, jnp.where(z < s, z, far))
    owner = z == s
    dx, dy = x != z % 2, y != z // 2
    on_x = dx & jnp.logical_not(dy)
    on_y = dy & jnp.logical_not(dx)
    on_d = dx & dy
    apart = jnp.maximum(z - s, s - z)
    key_step = jnp.where(apart == nz - 1, nchunks + 2, nchunks)

    def gradient_columns(j):
        for i in range(2, 6):
            token_arrival(j, i).wait_recv()
        at = pl.ds(pl.multiple_of(j * COLS, COLS), COLS)
        theirs = pl.ds(pl.multiple_of((1 - core) * wrows, wrows), wrows)
        mine = pl.ds(pl.multiple_of(core * wrows, wrows), wrows)
        pwo[j] = dot_nn(gkt[theirs, :], tall[:, at]).astype(BF16)
        half_copy(j).start()
        acc[j] = dot_nn(gkt[mine, :], tall[:, at])

    def sum_line(j):
        half_copy(j).wait_recv()
        acc[j] = acc[j] + rp[j].astype(F32)

        @pl.when((z >= s) & (z < nz - 1))
        def _():
            line_copy(j, 1, down).wait_recv()
            acc[j] = acc[j] + lrecv[1, j].astype(F32)

        @pl.when((z <= s) & (z > 0))
        def _():
            line_copy(j, 0, up).wait_recv()
            acc[j] = acc[j] + lrecv[0, j].astype(F32)

        @pl.when(owner)
        def _():
            fin[j] = acc[j].astype(BF16)
            cast_copy(j, 0, xn).start()
            cast_copy(j, 1, yn).start()

        @pl.when(jnp.logical_not(owner))
        def _():
            lsend[j] = acc[j].astype(BF16)

        @pl.when(z > s)
        def _():
            line_copy(j, 1, down).start()

        @pl.when(z < s)
        def _():
            line_copy(j, 0, up).start()

    def make_keys():
        for p in range(pieces):
            pair_arrival(s, p).wait_recv()
        left = pl.ds(pl.multiple_of(s * feats, feats), feats)

        def tile(i, _):
            at = pl.ds(pl.multiple_of(i * TILE, TILE), TILE)
            keys[at, :] = dot_nt(tall[at, :], wall[left, :]).astype(BF16)
            return 0

        lax.fori_loop(0, seq_len // TILE, tile, 0)

    def gq_copy(n):
        span = BLOCK * heads
        at = pl.ds(pl.multiple_of(n * span, span), span)
        return pltpu.make_async_copy(gq4.at[at, :], gq_out.at[at, :], gq_store.at[n])

    def gv_copy(n):
        span = BLOCK * heads * parts
        at = pl.ds(pl.multiple_of(n * span, span), span)
        return pltpu.make_async_copy(gv8.at[at, :], gv_out.at[at, :], gv_store.at[n])

    def query_block(n):
        at = pl.ds(pl.multiple_of(n * BLOCK, BLOCK), BLOCK)
        cosine, sine = cosv[at, :], sinv[at, :]
        for h in range(heads):
            kc, vc = slice(h * kw, (h + 1) * kw), slice(h * vw, (h + 1) * vw)
            key = keys[at, kc].astype(F32)
            rk = ((key * cosine + pltpu.roll(key, half, 1) * sine) * factor).astype(BF16)
            q, v, c = rq[at, kc], vals[at, vc], call[at, vc]
            state = entering[h]
            grad = dot_nn(mix[at, h * BLOCK:(h + 1) * BLOCK], rk)
            grad = grad + rising[h] * dot_nt(c, state.astype(BF16))
            xs[pl.ds(h, BLOCK, stride=heads), :] = (
                grad * cosine - pltpu.roll(grad, half, 1) * sine
            )
            scores = (dot_nt(q, rk) * within[h]).astype(BF16)
            fall = falling[h]
            inner = dot_tn(scores, c)
            outer = dot_nn(rk, held[h * nblocks + n])
            for i in range(parts):
                lane = slice(i * LANES, (i + 1) * LANES)
                ys[pl.ds(i * heads + h, BLOCK, stride=heads * parts), :] = (
                    inner[:, lane] + fall * outer[:, lane]
                )
            decayed = (rk.astype(F32) * fall).astype(BF16)
            entering[h] = state * carry[h, 0:1, :] + dot_tn(decayed, v)
        span = BLOCK * heads
        gq4[pl.ds(pl.multiple_of(n * span, span), span), :] = xs[...].astype(BF16)
        span = BLOCK * heads * parts
        gv8[pl.ds(pl.multiple_of(n * span, span), span), :] = ys[...].astype(BF16)
        gq_copy(n).start()
        gv_copy(n).start()

    def token_gradient():
        for j in range(1, nsp):
            gk_copy(j, (s - j + nsp) % nsp).wait_recv()
        gkall[:, pl.ds(pl.multiple_of(s * feats, feats), feats)] = gk[
            pl.ds(pl.multiple_of(s * rows, rows), rows), :
        ]
        for zb in range(nz):
            @pl.when(zb != s)
            def _():
                for p in range(pieces):
                    pair_arrival(zb, p).wait_recv()

        def tile(i, _):
            at = pl.ds(pl.multiple_of(i * TILE, TILE), TILE)
            gt[:, at] = dot_nn(gkall[...], wall[:, at]).astype(BF16)
            return 0

        lax.fori_loop(0, width // TILE, tile, 0)
        pltpu.make_async_copy(gt, gt_out, gt_store.at[0]).start()

    last = nchunks + 3 + (nz - 1)

    def turn(t, _):
        @pl.when(t + 1 < nchunks)
        def _():
            for i in range(4):
                token_send(t + 1, i).start()

        @pl.when(t < nchunks)
        def _():
            token_arrival(t, 0).wait_recv()
            token_send(t, 4).start()
            token_arrival(t, 1).wait_recv()
            token_send(t, 5).start()

        @pl.when(t == nchunks - 1)
        def _():
            for j in range(1, nsp):
                gk_copy(j, s).start()

        @pl.when((t >= 1) & (t <= nchunks))
        def _():
            gradient_columns(t - 1)

        j = t - 2 - behind

        @pl.when((j >= 0) & (j < nchunks))
        def _():
            sum_line(j)

        jx = t - 3 - far

        @pl.when(on_x & (jx >= 0) & (jx < nchunks))
        def _():
            cast_copy(jx, 0, xn).wait_recv()
            cast_copy(jx, 0, yn).start()

        @pl.when(on_y & (jx >= 0) & (jx < nchunks))
        def _():
            cast_copy(jx, 1, yn).wait_recv()
            cast_copy(jx, 1, xn).start()

        jd = t - 4 - far

        @pl.when(on_d & (jd >= 0) & (jd < nchunks))
        def _():
            cast_copy(jd, 0, yn).wait_recv()
            cast_copy(jd, 0, xn).start()
            cast_copy(jd, 1, xn).wait_recv()
            cast_copy(jd, 1, yn).start()

        @pl.when((t >= 1) & (t <= pieces))
        def _():
            relay(2, t - 1)

        @pl.when((t >= nchunks + 3 - pieces) & (t < nchunks + 3))
        def _():
            relay(3, t - (nchunks + 3 - pieces))

        @pl.when(t == key_step)
        def _():
            make_keys()

        n = (t - key_step - 1) * 2

        @pl.when((n >= 0) & (n < nblocks))
        def _():
            query_block(n)
            query_block(n + 1)

        @pl.when(t == last - 1)
        def _():
            token_gradient()

        return 0

    lax.fori_loop(0, last + 1, turn, 0)

    def gw_copy(j):
        at = pl.ds(pl.multiple_of(j * COLS, COLS), COLS)
        return pltpu.make_async_copy(fin.at[j], gw_out.at[:, at], gw_store.at[j])

    def finish(j, _):
        @pl.when(on_x)
        def _():
            cast_copy(j, 1, xn).wait_recv()

        @pl.when(on_y)
        def _():
            cast_copy(j, 0, yn).wait_recv()

        gw_copy(j).start()
        return 0

    lax.fori_loop(0, nchunks, finish, 0)

    for h in range(heads):
        for j in range(1, nsp):
            cot_copy(j, h, s).wait_send()
    for j in range(1, nsp):
        gk_copy(j, s).wait_send()

    def settle(j, _):
        for i in range(6):
            token_send(j, i).wait_send()
        half_copy(j).wait_send()

        @pl.when(jnp.logical_not(owner))
        def _():
            line_copy(j, 0, partner).wait_send()

        @pl.when(jnp.logical_not(on_y))
        def _():
            cast_copy(j, 0, xn).wait_send()

        @pl.when(jnp.logical_not(on_x))
        def _():
            cast_copy(j, 1, xn).wait_send()

        gw_copy(j).wait()
        return 0

    lax.fori_loop(0, nchunks, settle, 0)

    for p in range(pieces):
        for d in range(nz - 1):
            @pl.when((z >= d) & (z < nz - 1))
            def _():
                up_copy(d, p).wait_send()

            @pl.when((z + d < nz) & (z > 0))
            def _():
                down_copy(d, p).wait_send()

        for zb in range(nz):
            pair_copy(zb, p).wait_send()

    def drain(n, _):
        gq_copy(n).wait()
        gv_copy(n).wait()
        return 0

    lax.fori_loop(0, nblocks, drain, 0)
    pltpu.make_async_copy(gt, gt_out, gt_store.at[0]).wait()


def whole(tokens, weight, queries, values, cotan, decay, nsp, ndp, heads):
    nz = ndp // CORES
    rows, width = tokens.shape
    wrows = weight.shape[0]
    seq_len = rows * nsp
    kw = queries.shape[1]
    feats = heads * kw
    cwidth = cotan.shape[1] // nsp
    vw = cwidth // heads
    nblocks = seq_len // BLOCK
    nchunks = width // COLS
    cosine, sine = rotation_tables(seq_len, kw // 2)
    dma = pltpu.SemaphoreType.DMA
    anywhere = pl.BlockSpec(memory_space=pl.ANY)

    def buffer(*shape):
        return pltpu.VMEM(shape, BF16)

    def wide(*shape):
        return pltpu.VMEM(shape, F32)

    return pl.pallas_call(
        functools.partial(whole_kernel, nsp, nz, heads),
        in_specs=[pl.BlockSpec(memory_space=pltpu.SMEM)] + [anywhere] * 7,
        out_specs=[anywhere] * 4,
        out_shape=[
            jax.ShapeDtypeStruct((rows, width), BF16),
            jax.ShapeDtypeStruct(queries.shape, BF16),
            jax.ShapeDtypeStruct(values.shape, BF16),
            jax.ShapeDtypeStruct((wrows, width), BF16),
        ],
        scratch_shapes=[
            buffer(rows, nsp * cwidth),
            buffer(seq_len, width),
            buffer(wrows * ndp, width),
            buffer(seq_len, cwidth),
            buffer(*queries.shape),
            buffer(*values.shape),
            wide(seq_len, kw),
            wide(seq_len, kw),
            buffer(seq_len, feats),
            buffer(seq_len, cwidth),
            buffer(seq_len, heads * BLOCK),
            buffer(heads * nblocks, kw, vw),
            buffer(seq_len, feats),
            buffer(feats, seq_len),
            buffer(rows, nsp * feats),
            buffer(seq_len, feats),
            buffer(*queries.shape),
            buffer(*values.shape),
            buffer(rows, width),
            wide(nchunks, wrows, COLS),
            buffer(nchunks, wrows, COLS),
            buffer(nchunks, wrows, COLS),
            buffer(2, nchunks, wrows, COLS),
            buffer(nchunks, wrows, COLS),
            buffer(nchunks, wrows, COLS),
            wide(BLOCK * heads, kw),
            wide(BLOCK * heads * (vw // LANES), LANES),
            wide(heads, BLOCK, BLOCK),
            wide(heads, BLOCK, kw),
            wide(heads, BLOCK, kw),
            wide(heads, 8, vw),
            wide(heads, kw, vw),
            dma((8,)),
            dma((nsp * heads,)), dma((nsp * heads,)),
            dma((6 * nchunks,)), dma((6 * nchunks,)),
            dma((nz * heads,)), dma((nz * heads,)),
            dma((nz * heads,)), dma((nz * heads,)),
            dma((nz * heads,)), dma((nz * heads,)),
            dma((nsp,)), dma((nsp,)),
            dma((nchunks,)), dma((nchunks,)),
            dma((nchunks,)), dma((2 * nchunks,)),
            dma((2 * nchunks,)), dma((2 * nchunks,)),
            dma((nblocks,)), dma((nblocks,)), dma((nchunks,)), dma((1,)),
        ],
        compiler_params=pltpu.CompilerParams(
            has_side_effects=True, vmem_limit_bytes=VMEM_LIMIT, collective_id=0
        ),
        name="whole",
    )(decay, tokens, weight, queries, values, cotan, jnp.asarray(cosine), jnp.asarray(sine))


def gather_general(tokens, weight, cotan):
    gathered = lax.all_gather(weight, "dp", axis=0, tiled=True)
    rows = gathered.shape[0] // lax.axis_size("sp")
    chosen = lax.dynamic_slice_in_dim(gathered, lax.axis_index("sp") * rows, rows)
    return (
        lax.all_gather(tokens, "sp", axis=0, tiled=True),
        chosen,
        lax.all_to_all(cotan, "sp", split_axis=1, concat_axis=0, tiled=True),
    )


def scatter_general(partial_tokens, partial_weight):
    grad_tokens = lax.psum_scatter(
        partial_tokens, "sp", scatter_dimension=0, tiled=True
    ).astype(BF16)
    owned = lax.psum_scatter(
        partial_weight, "dp", scatter_dimension=0, tiled=True
    )
    everything = lax.all_gather(owned, ("sp", "dp"), axis=0, tiled=True)
    rows = everything.shape[0] // lax.axis_size("dp")
    return grad_tokens, lax.dynamic_slice_in_dim(
        everything, lax.axis_index("dp") * rows, rows
    )


def body(nsp, ndp, tokens, key_weight, queries, values, cotangent, log_decay):
    seq_len, heads, kw = queries.shape[1:]
    vw = values.shape[3]
    if nsp == 4 and ndp == CORES * nsp and kw == BLOCK:
        parts = vw // LANES
        flat = values.reshape(seq_len, heads, parts, LANES).transpose(0, 2, 1, 3)
        grad_tokens, grad_query, grad_value, weight_grad = whole(
            tokens[0], key_weight, queries.reshape(-1, kw), flat.reshape(-1, LANES),
            cotangent[0], log_decay, nsp, ndp, heads,
        )
        grad_value = grad_value.reshape(seq_len, parts, heads, LANES).transpose(0, 2, 1, 3)
        weight_grad = weight_grad.astype(F32)
    else:
        all_tokens, weight, cotan = gather_general(tokens[0], key_weight, cotangent[0])
        keys = dot_nt(all_tokens, weight).astype(BF16)
        grad_query, grad_key, _, grad_value = retention_backward(
            queries.reshape(seq_len, -1), keys, values.reshape(seq_len, -1), cotan, log_decay, heads
        )
        grad_tokens, weight_grad = scatter_general(
            dot_nn(grad_key, weight), dot_tn(grad_key, all_tokens)
        )
    return (
        grad_tokens[None],
        grad_query.reshape(queries.shape),
        grad_value.reshape(values.shape),
        weight_grad,
    )


def solution(mesh):
    return jax.shard_map(
        functools.partial(body, mesh.shape["sp"], mesh.shape["dp"]),
        mesh=mesh,
        in_specs=(
            P("dp", "sp", None),
            P("dp", None),
            P("dp", None, "sp", None),
            P("dp", None, "sp", None),
            P("dp", "sp", None),
            P(),
        ),
        out_specs=(
            P("dp", "sp", None),
            P("dp", None, "sp", None),
            P("dp", None, "sp", None),
            P("dp", None),
        ),
        check_vma=False,
    )
```

time: 161 us -> 131 us (0.81)
  the two profiles are of different devices: /device:TPU:0 before, /device:TPU:3 now
where the time goes in v1:
time: 131 us; the launch traced here: 130 us
  Pallas kernels  124 us (95%)
  local copies, waits for them, and re-layouts  3.34 us (3%)
  other arithmetic  2.94 us (2%)
    pallas_call x1, Pallas kernels, whole(): pl.pallas_call(functools.partial(whole_kernel, nsp, nz, heads), in_specs=...  124 us
    unnamed x9, local copies, waits for them, and re-layouts  3.34 us
    convert_element_type x1, other arithmetic, body(): weight_grad = weight_grad.astype(F32)  2.94 us

profile of v1, /device:TPU:3, one launch (start us, length us, event | category | flops | bytes accessed | tf_op | source)
XLA Modules:
  0.0 130.4 jit_solution(237660775578354765)
XLA Ops:
  0.6 123.5 %whole.1 = (bf16[256,2048]{1,0:T(8,128)(2,1)}, bf16[4096,128]{1,0:T(8,128)(2,1)}, bf16[8192,128]{1,0:T(8,128)(2,1)}, bf16[256,2048]{1,0:T(8,128)(2,1)}) custom-call(f32[16]{0:T(128)} %decay_ref.1, bf16[256,2048]{1,0:T(8,128)(2,1)} %bitcast.18, bf16[256,2048]{1,0:T(8,128)(2,1)} %w_in.1, bf16[4096,128]{1,0:T(8,128)(2,1)} %bitcast.19, ...), custom_call_target="tpu_custom_call" | custom-call | tf_op jit(solution)/shard_map/whole/pallas_call | solution.py:680
  124.1 0.0 copy-start.2
  124.2 0.0 copy-start.1
  124.2 2.9 %convert_element_type.3 = f32[256,2048]{1,0:T(8,128)} convert(bf16[256,2048]{1,0:T(8,128)(2,1)} %get-tuple-element.11) | non-fusion elementwise | flops 524288 | bytes 3145728 | tf_op jit(solution)/shard_map/convert_element_type | solution.py:778
  127.1 0.0 copy-done.2
  127.1 0.0 copy-start
  127.1 1.0 copy.17
  128.1 0.0 copy-done.1
  128.1 1.0 copy.18
  129.1 0.1 copy-done
  129.1 1.3 %copy.19 = bf16[1,1024,4,256]{3,2,1,0:T(4,128)(2,1)} copy(bf16[1,1024,4,256]{3,2,1,0:T(4,128)(2,1)S(1)} %bitcast.15) | data formatting | bytes 4194304
Async XLA Ops:
  124.1 3.0 %copy-start.2 = (bf16[256,2048]{1,0:T(8,128)(2,1)S(1)}, bf16[256,2048]{1,0:T(8,128)(2,1)}, u32[]{:S(2)}) copy-start(bf16[256,2048]{1,0:T(8,128)(2,1)} %get-tuple-element.8) | copy-start | bytes 3145732
  124.2 3.9 %copy-start.1 = (bf16[4096,128]{1,0:T(8,128)(2,1)S(1)}, bf16[4096,128]{1,0:T(8,128)(2,1)}, u32[]{:S(2)}) copy-start(bf16[4096,128]{1,0:T(8,128)(2,1)} %get-tuple-element.9) | copy-start | bytes 3145732
  127.1 2.0 %copy-start = (bf16[8192,128]{1,0:T(8,128)(2,1)S(1)}, bf16[8192,128]{1,0:T(8,128)(2,1)}, u32[]{:S(2)}) copy-start(bf16[8192,128]{1,0:T(8,128)(2,1)} %get-tuple-element.10) | copy-start | bytes 6291460

commit v2 on v1

--- a/solution.py
+++ b/solution.py
@@ -142,15 +142,27 @@
     barrier = pltpu.get_barrier_semaphore()
     others = [{"dp": z * CORES + 1 - core}]
     others += [{"sp": (s + j) % nsp} for j in range(1, nsp)]
-    others += [{"dp": (z + j) % nz * CORES + core} for j in range(1, nz)]
     for other in others:
         pl.semaphore_signal(barrier, inc=1, device_id=other, device_id_type=MESH)
-    pl.semaphore_wait(barrier, len(others))
+
+    @pl.when(z > 0)
+    def _():
+        below = {"dp": (z - 1) * CORES + core}
+        pl.semaphore_signal(barrier, inc=1, device_id=below, device_id_type=MESH)
+
+    @pl.when(z < nz - 1)
+    def _():
+        above = {"dp": (z + 1) * CORES + core}
+        pl.semaphore_signal(barrier, inc=1, device_id=above, device_id_type=MESH)
+
+    ends = jnp.where(z > 0, 1, 0) + jnp.where(z < nz - 1, 1, 0)
+    pl.semaphore_wait(barrier, len(others) + ends)
 
 
 TILE = 256
 LANES = 128
 COLS = 256
+HOP = 1
 
 
 def whole_kernel(
@@ -158,10 +170,10 @@
     decay_ref, tok_in, w_in, q_in, v_in, cot_in, cos_in, sin_in,
     gt_out, gq_out, gv_out, gw_out,
     cotv, tall, wall, call, q4, v8, cosv, sinv, rq, vals, mix, held, gk, gkt, gkall,
-    keys, gq4, gv8, gt, acc, pwo, rp, lrecv, lsend, fin, xs, ys,
+    keys, gq4, gv8, gt, gtf, acc, pwo, rp, lrecv, lsend, fin, xs, ys,
     within, rising, falling, carry, entering,
     load, cot_send, cot_recv, tok_send, tok_recv,
-    up_send, up_recv, down_send, down_recv, pair_send, pair_recv,
+    up_send, up_recv, down_send, down_recv, pair_send, pair_recv, side_send, side_recv,
     gk_send, gk_recv, half_send, half_recv, line_send, line_recv,
     cast_send, cast_recv, gq_store, gv_store, gw_store, gt_store,
 ):
@@ -188,6 +200,23 @@
     pieces = heads
     prow = wrows // pieces
 
+    far = jnp.maximum(z, nz - 1 - z)
+    behind = jnp.where(z > s, nz - 1 - z, jnp.where(z < s, z, far))
+    owner = z == s
+    dx, dy = x != z % 2, y != z // 2
+    on_x = dx & jnp.logical_not(dy)
+    on_y = dy & jnp.logical_not(dx)
+    on_d = dx & dy
+    edge = (z == 0) | (z == nz - 1)
+    corner = owner & edge
+    side_x, side_y = on_x & edge, on_y & edge
+    apart = jnp.maximum(z - s, s - z)
+    opposite = apart == nz - 1
+    yields_up = (s == 0) & (z == nz - 2)
+    yields_down = (s == nz - 1) & (z == 1)
+    farthest = jnp.where(z < nz // 2, nz - 1, 0)
+    tardy = jnp.where(opposite, jnp.where(z == 0, nz - 2, 1), farthest)
+
     loads = [
         pltpu.make_async_copy(cot_in, cotv, load.at[0]),
         pltpu.make_async_copy(w_in, wall.at[pl.ds(pl.multiple_of(k * wrows, wrows), wrows), :], load.at[1]),
@@ -205,14 +234,20 @@
         copy.start()
     greet(nsp, nz, s, z, core)
 
+    def received(ref, sem):
+        remote(ref, ref, load.at[0], sem, partner).wait_recv()
+
+    def sent(ref, sem):
+        remote(ref, ref, sem, load.at[0], partner).wait_send()
+
     def cot_copy(j, h, source):
         peer = (s + j) % nsp
         columns = pl.ds(pl.multiple_of(peer * cwidth + h * vw, vw), vw)
         to = call.at[
             pl.ds(pl.multiple_of(source * rows, rows), rows), pl.ds(pl.multiple_of(h * vw, vw), vw)
         ]
-        i = j * heads + h
-        return remote(cotv.at[:, columns], to, cot_send.at[i], cot_recv.at[i], {"sp": peer})
+        i = (j - 1) * heads + h
+        return remote(cotv.at[:, columns], to, cot_send.at[0], cot_recv.at[i], {"sp": peer})
 
     loads[0].wait()
     for h in range(heads):
@@ -225,27 +260,18 @@
 
     def up_copy(d, p):
         ref, i = piece(z - d, core, p), d * pieces + p
-        return remote(ref, ref, up_send.at[i], up_recv.at[i], up)
+        return remote(ref, ref, up_send.at[d], up_recv.at[i], up)
 
     def down_copy(d, p):
         ref, i = piece(z + d, core, p), d * pieces + p
-        return remote(ref, ref, down_send.at[i], down_recv.at[i], down)
-
-    def up_arrival(d, p):
-        ref, i = piece(z - d, core, p), (d - 1) * pieces + p
-        return remote(ref, ref, up_send.at[i], up_recv.at[i], partner)
-
-    def down_arrival(d, p):
-        ref, i = piece(z + d, core, p), (d - 1) * pieces + p
-        return remote(ref, ref, down_send.at[i], down_recv.at[i], partner)
+        return remote(ref, ref, down_send.at[d], down_recv.at[i], down)
 
     def pair_copy(zb, p):
-        ref, i = piece(zb, core, p), zb * pieces + p
-        return remote(ref, ref, pair_send.at[i], pair_recv.at[i], partner)
-
-    def pair_arrival(zb, p):
-        ref, i = piece(zb, 1 - core, p), zb * pieces + p
-        return remote(ref, ref, pair_send.at[i], pair_recv.at[i], partner)
+        ref = piece(zb, core, p)
+        return remote(ref, ref, pair_send.at[0], pair_recv.at[zb], partner)
+
+    def pair_wait(zb):
+        received(wall.at[:wrows, :], pair_recv.at[zb])
 
     loads[1].wait()
     for p in range(pieces):
@@ -259,32 +285,128 @@
 
         pair_copy(z, p).start()
 
-    def relay(d, p):
-        @pl.when(z >= d)
-        def _():
-            up_arrival(d, p).wait_recv()
-            if d < nz - 1:
-                @pl.when(z < nz - 1)
-                def _():
-                    up_copy(d, p).start()
-            pair_copy(z - d, p).start()
-
-        @pl.when(z + d < nz)
-        def _():
-            down_arrival(d, p).wait_recv()
-            if d < nz - 1:
-                @pl.when(z > 0)
-                def _():
-                    down_copy(d, p).start()
-            pair_copy(z + d, p).start()
+    def goes_up(d):
+        return (z >= d) & (z < nz - 1 if d < nz - 2 else (z < nz - 1) & (s != nz - 1))
+
+    def goes_down(d):
+        return (z + d < nz) & (z > 0 if d < nz - 2 else (z > 0) & (s != 0))
+
+    def side_copy(p, target):
+        ref = piece(nz - 1 - z, core, p)
+        return remote(ref, ref, side_send.at[0], side_recv.at[0], {"sp": target})
+
+    def rise_of(d, p):
+        received(piece(z - d, core, p), up_recv.at[(d - 1) * pieces + p])
+        pair_copy(z - d, p).start()
+
+    def fall_of(d, p):
+        received(piece(z + d, core, p), down_recv.at[(d - 1) * pieces + p])
+        pair_copy(z + d, p).start()
+
+    def relay_first(p):
+        @pl.when(z > 0)
+        def _():
+            rise_of(1, p)
+
+        @pl.when(goes_up(1) & (z >= s) & prompt(p, yields_up))
+        def _():
+            up_copy(1, p).start()
+
+        @pl.when(z < nz - 1)
+        def _():
+            fall_of(1, p)
+
+        @pl.when(goes_down(1) & (z <= s) & prompt(p, yields_down))
+        def _():
+            down_copy(1, p).start()
+
+    def relay_inward(p):
+        @pl.when(goes_up(1) & (z < s))
+        def _():
+            up_copy(1, p).start()
+
+        @pl.when(goes_down(1) & (z > s))
+        def _():
+            down_copy(1, p).start()
+
+    def relay_second(p):
+        @pl.when((z >= 2) & (z > s))
+        def _():
+            rise_of(2, p)
+
+        @pl.when(goes_up(2) & (z > s))
+        def _():
+            up_copy(2, p).start()
+
+        @pl.when((z + 2 < nz) & (z < s))
+        def _():
+            fall_of(2, p)
+
+        @pl.when(goes_down(2) & (z < s))
+        def _():
+            down_copy(2, p).start()
+
+    def take_inward(p):
+        @pl.when((z >= 2) & (z <= s))
+        def _():
+            rise_of(2, p)
+
+        @pl.when(goes_up(2) & (z == s))
+        def _():
+            up_copy(2, p).start()
+
+        @pl.when((z + 2 < nz) & (z >= s))
+        def _():
+            fall_of(2, p)
+
+        @pl.when(goes_down(2) & (z == s))
+        def _():
+            down_copy(2, p).start()
+
+    def relay_third(p):
+        @pl.when((z == nz - 1) & (s != z))
+        def _():
+            rise_of(3, p)
+
+        @pl.when((z == 0) & (s != z))
+        def _():
+            fall_of(3, p)
+
+        @pl.when(side_x & (p < pieces // 2))
+        def _():
+            side_copy(p, xn).start()
+
+        @pl.when(side_y & (p >= pieces // 2))
+        def _():
+            side_copy(p, yn).start()
+
+    def prompt(p, yields):
+        return jnp.logical_not(yields & (p > 0))
+
+    def relay_rest():
+        for p in range(1, pieces):
+            @pl.when(yields_up)
+            def _():
+                up_copy(1, p).start()
+
+            @pl.when(yields_down)
+            def _():
+                down_copy(1, p).start()
+
+    def take_side():
+        @pl.when(corner)
+        def _():
+            received(wall.at[:wrows, :], side_recv.at[0])
+            for p in range(pieces):
+                pair_copy(nz - 1 - z, p).start()
 
     def token(j, i, who, h, target):
         at = tall.at[
             pl.ds(pl.multiple_of(who * rows + h * hrows, hrows), hrows),
             pl.ds(pl.multiple_of(j * COLS, COLS), COLS),
         ]
-        n = j * 6 + i
-        return remote(at, at, tok_send.at[n], tok_recv.at[n], {"sp": target})
+        n = 2 * j + (0 if i < 2 else 1)
+        return remote(at, at, tok_send.at[0], tok_recv.at[n], {"sp": target})
 
     def token_send(j, i):
         who, h, target = [
@@ -292,15 +414,14 @@
         ][i]
         return token(j, i, who, h, target)
 
-    def token_arrival(j, i):
-        who, h, target = [
-            (xn, 0, xn), (yn, 1, yn), (xn, 1, xn), (yn, 0, yn), (diagonal, 0, yn), (diagonal, 1, xn)
-        ][i]
-        return token(j, i, who, h, target)
+    def token_wait(j, count, n):
+        at = pl.ds(pl.multiple_of(j * COLS, COLS), COLS)
+        received(tall.at[:count * hrows, at], tok_recv.at[2 * j + n])
 
     loads[2].wait()
-    for i in range(4):
-        token_send(0, i).start()
+    for j in range(2):
+        for i in range(4):
+            token_send(j, i).start()
     for copy in loads[3:]:
         copy.wait()
 
@@ -325,7 +446,7 @@
     lax.fori_loop(0, nblocks, prepare, 0)
 
     def key_head(h, _):
-        relay(1, h)
+        relay_first(h)
         for j in range(1, nsp):
             cot_copy(j, h, (s - j + nsp) % nsp).wait_recv()
         kc = pl.ds(pl.multiple_of(h * kw, kw), kw)
@@ -367,36 +488,25 @@
         to = gkall.at[:, pl.ds(pl.multiple_of(source * feats, feats), feats)]
         return remote(
             gk.at[pl.ds(pl.multiple_of(peer * rows, rows), rows), :], to,
-            gk_send.at[j], gk_recv.at[j], {"sp": peer},
+            gk_send.at[0], gk_recv.at[0], {"sp": peer},
         )
 
     def half_copy(j):
-        return remote(pwo.at[j], rp.at[j], half_send.at[j], half_recv.at[j], partner)
+        return remote(pwo.at[j], rp.at[j], half_send.at[0], half_recv.at[j], partner)
 
     def line_copy(j, side, target):
         return remote(
-            lsend.at[j], lrecv.at[side, j], line_send.at[j],
+            lsend.at[j], lrecv.at[side, j], line_send.at[0],
             line_recv.at[side * nchunks + j], target,
         )
 
-    def cast_copy(j, h, target):
+    def cast_copy(j, h, target, last_leg=False):
         ref = fin.at[j, pl.ds(h * (wrows // 2), wrows // 2), :]
-        i = 2 * j + h
-        return remote(ref, ref, cast_send.at[i], cast_recv.at[i], {"sp": target})
-
-    far = jnp.maximum(z, nz - 1 - z)
-    behind = jnp.where(z > s, nz - 1 - z, jnp.where(z < s, z, far))
-    owner = z == s
-    dx, dy = x != z % 2, y != z // 2
-    on_x = dx & jnp.logical_not(dy)
-    on_y = dy & jnp.logical_not(dx)
-    on_d = dx & dy
-    apart = jnp.maximum(z - s, s - z)
-    key_step = jnp.where(apart == nz - 1, nchunks + 2, nchunks)
+        sem = cast_recv.at[nchunks if last_leg else j]
+        return remote(ref, ref, cast_send.at[0], sem, {"sp": target})
 
     def gradient_columns(j):
-        for i in range(2, 6):
-            token_arrival(j, i).wait_recv()
+        token_wait(j, 4, 1)
         at = pl.ds(pl.multiple_of(j * COLS, COLS), COLS)
         theirs = pl.ds(pl.multiple_of((1 - core) * wrows, wrows), wrows)
         mine = pl.ds(pl.multiple_of(core * wrows, wrows), wrows)
@@ -437,8 +547,7 @@
             line_copy(j, 0, up).start()
 
     def make_keys():
-        for p in range(pieces):
-            pair_arrival(s, p).wait_recv()
+        pair_wait(s)
         left = pl.ds(pl.multiple_of(s * feats, feats), feats)
 
         def tile(i, _):
@@ -451,12 +560,12 @@
     def gq_copy(n):
         span = BLOCK * heads
         at = pl.ds(pl.multiple_of(n * span, span), span)
-        return pltpu.make_async_copy(gq4.at[at, :], gq_out.at[at, :], gq_store.at[n])
+        return pltpu.make_async_copy(gq4.at[at, :], gq_out.at[at, :], gq_store.at[0])
 
     def gv_copy(n):
         span = BLOCK * heads * parts
         at = pl.ds(pl.multiple_of(n * span, span), span)
-        return pltpu.make_async_copy(gv8.at[at, :], gv_out.at[at, :], gv_store.at[n])
+        return pltpu.make_async_copy(gv8.at[at, :], gv_out.at[at, :], gv_store.at[0])
 
     def query_block(n):
         at = pl.ds(pl.multiple_of(n * BLOCK, BLOCK), BLOCK)
@@ -490,40 +599,44 @@
         gq_copy(n).start()
         gv_copy(n).start()
 
-    def token_gradient():
-        for j in range(1, nsp):
-            gk_copy(j, (s - j + nsp) % nsp).wait_recv()
+    def gather_keys():
+        received(gkall.at[:, :(nsp - 1) * feats], gk_recv.at[0])
         gkall[:, pl.ds(pl.multiple_of(s * feats, feats), feats)] = gk[
             pl.ds(pl.multiple_of(s * rows, rows), rows), :
         ]
         for zb in range(nz):
-            @pl.when(zb != s)
+            @pl.when((zb != s) & (zb != tardy))
             def _():
-                for p in range(pieces):
-                    pair_arrival(zb, p).wait_recv()
-
-        def tile(i, _):
-            at = pl.ds(pl.multiple_of(i * TILE, TILE), TILE)
-            gt[:, at] = dot_nn(gkall[...], wall[:, at]).astype(BF16)
-            return 0
-
-        lax.fori_loop(0, width // TILE, tile, 0)
-        pltpu.make_async_copy(gt, gt_out, gt_store.at[0]).start()
-
-    last = nchunks + 3 + (nz - 1)
+                pair_wait(zb)
+
+    def gt_copy(i):
+        at = pl.ds(pl.multiple_of(i * TILE, TILE), TILE)
+        return pltpu.make_async_copy(gt.at[:, at], gt_out.at[:, at], gt_store.at[0])
+
+    def block_product(zb, at):
+        inner = pl.ds(pl.multiple_of(zb * feats, feats), feats)
+        return dot_nn(gkall[:, inner], wall[inner, at])
+
+    def token_gradient(i):
+        at = pl.ds(pl.multiple_of(i * TILE, TILE), TILE)
+        total = block_product((tardy + 1) % nz, at)
+        for j in range(2, nz):
+            total = total + block_product((tardy + j) % nz, at)
+        gtf[i] = total
+
+    last = nchunks + 1 + (nz + 1) * HOP
 
     def turn(t, _):
-        @pl.when(t + 1 < nchunks)
+        @pl.when(t < nchunks)
+        def _():
+            token_wait(t, 2, 0)
+            token_send(t, 4).start()
+            token_send(t, 5).start()
+
+        @pl.when(t + 2 < nchunks)
         def _():
             for i in range(4):
-                token_send(t + 1, i).start()
-
-        @pl.when(t < nchunks)
-        def _():
-            token_arrival(t, 0).wait_recv()
-            token_send(t, 4).start()
-            token_arrival(t, 1).wait_recv()
-            token_send(t, 5).start()
+                token_send(t + 2, i).start()
 
         @pl.when(t == nchunks - 1)
         def _():
@@ -534,126 +647,146 @@
         def _():
             gradient_columns(t - 1)
 
-        j = t - 2 - behind
+        j = t - 2 - behind * HOP
 
         @pl.when((j >= 0) & (j < nchunks))
         def _():
             sum_line(j)
 
-        jx = t - 3 - far
+        jx = t - 2 - (far + 1) * HOP
 
         @pl.when(on_x & (jx >= 0) & (jx < nchunks))
         def _():
-            cast_copy(jx, 0, xn).wait_recv()
+            received(fin.at[jx, :wrows // 2, :], cast_recv.at[jx])
             cast_copy(jx, 0, yn).start()
 
         @pl.when(on_y & (jx >= 0) & (jx < nchunks))
         def _():
-            cast_copy(jx, 1, yn).wait_recv()
+            received(fin.at[jx, wrows // 2:, :], cast_recv.at[jx])
             cast_copy(jx, 1, xn).start()
 
-        jd = t - 4 - far
+        jd = t - 2 - (far + 2) * HOP
 
         @pl.when(on_d & (jd >= 0) & (jd < nchunks))
         def _():
-            cast_copy(jd, 0, yn).wait_recv()
-            cast_copy(jd, 0, xn).start()
-            cast_copy(jd, 1, xn).wait_recv()
-            cast_copy(jd, 1, yn).start()
-
-        @pl.when((t >= 1) & (t <= pieces))
-        def _():
-            relay(2, t - 1)
-
-        @pl.when((t >= nchunks + 3 - pieces) & (t < nchunks + 3))
-        def _():
-            relay(3, t - (nchunks + 3 - pieces))
-
-        @pl.when(t == key_step)
+            received(fin.at[jd], cast_recv.at[jd])
+            cast_copy(jd, 0, xn, True).start()
+            cast_copy(jd, 1, yn, True).start()
+
+        @pl.when(t < pieces)
+        def _():
+            relay_inward(t)
+
+        p = t - 2
+
+        @pl.when((p >= 0) & (p < pieces) & jnp.logical_not(opposite))
+        def _():
+            relay_second(p)
+
+        @pl.when((p >= 1) & (p <= pieces))
+        def _():
+            take_inward(p - 1)
+
+        p = t - jnp.where(opposite, pieces, nchunks + 1)
+
+        @pl.when((p >= 0) & (p < pieces))
+        def _():
+            relay_third(p)
+
+        p = t - nchunks - 1
+
+        @pl.when(opposite & (p >= 0) & (p < pieces))
+        def _():
+            relay_second(p)
+
+        @pl.when(t == pieces + 2)
+        def _():
+            relay_rest()
+
+        @pl.when(t == nchunks)
         def _():
             make_keys()
 
-        n = (t - key_step - 1) * 2
+        n = (t - nchunks - 1) * 2
 
         @pl.when((n >= 0) & (n < nblocks))
         def _():
             query_block(n)
             query_block(n + 1)
 
-        @pl.when(t == last - 1)
-        def _():
-            token_gradient()
+        i = t - tile_step
+
+        @pl.when(i == 0)
+        def _():
+            gather_keys()
+
+        @pl.when((i >= 0) & (i < ntiles // 2))
+        def _():
+            token_gradient(2 * i)
+            token_gradient(2 * i + 1)
 
         return 0
 
+    ntiles = width // TILE
+    tile_step = nchunks + HOP + 2
     lax.fori_loop(0, last + 1, turn, 0)
-
-    def gw_copy(j):
-        at = pl.ds(pl.multiple_of(j * COLS, COLS), COLS)
-        return pltpu.make_async_copy(fin.at[j], gw_out.at[:, at], gw_store.at[j])
-
-    def finish(j, _):
-        @pl.when(on_x)
-        def _():
-            cast_copy(j, 1, xn).wait_recv()
-
-        @pl.when(on_y)
-        def _():
-            cast_copy(j, 0, yn).wait_recv()
-
-        gw_copy(j).start()
+    take_side()
+
+    @pl.when(tardy != s)
+    def _():
+        pair_wait(tardy)
+
+    def complete(i, _):
+        at = pl.ds(pl.multiple_of(i * TILE, TILE), TILE)
+        gt[:, at] = (gtf[i] + block_product(tardy, at)).astype(BF16)
+        gt_copy(i).start()
         return 0
 
-    lax.fori_loop(0, nchunks, finish, 0)
-
-    for h in range(heads):
-        for j in range(1, nsp):
-            cot_copy(j, h, s).wait_send()
-    for j in range(1, nsp):
-        gk_copy(j, s).wait_send()
-
-    def settle(j, _):
-        for i in range(6):
-            token_send(j, i).wait_send()
-        half_copy(j).wait_send()
-
-        @pl.when(jnp.logical_not(owner))
-        def _():
-            line_copy(j, 0, partner).wait_send()
-
-        @pl.when(jnp.logical_not(on_y))
-        def _():
-            cast_copy(j, 0, xn).wait_send()
-
-        @pl.when(jnp.logical_not(on_x))
-        def _():
-            cast_copy(j, 1, xn).wait_send()
-
-        gw_copy(j).wait()
-        return 0
-
-    lax.fori_loop(0, nchunks, settle, 0)
-
-    for p in range(pieces):
-        for d in range(nz - 1):
-            @pl.when((z >= d) & (z < nz - 1))
-            def _():
-                up_copy(d, p).wait_send()
-
-            @pl.when((z + d < nz) & (z > 0))
-            def _():
-                down_copy(d, p).wait_send()
-
-        for zb in range(nz):
-            pair_copy(zb, p).wait_send()
-
-    def drain(n, _):
-        gq_copy(n).wait()
-        gv_copy(n).wait()
-        return 0
-
-    lax.fori_loop(0, nblocks, drain, 0)
+    lax.fori_loop(0, ntiles, complete, 0)
+
+    @pl.when(on_x | on_y)
+    def _():
+        received(fin.at[:nchunks // 2], cast_recv.at[nchunks])
+
+    gw_copy = pltpu.make_async_copy(fin, gw_out, gw_store.at[0])
+    gw_copy.start()
+
+    sent(cotv.at[:, :(nsp - 1) * cwidth], cot_send.at[0])
+    sent(tall.at[:6 * hrows, :], tok_send.at[0])
+    sent(gk.at[:(nsp - 1) * rows, :], gk_send.at[0])
+    sent(pwo, half_send.at[0])
+
+    @pl.when(jnp.logical_not(owner))
+    def _():
+        sent(lsend, line_send.at[0])
+
+    @pl.when(owner | on_d)
+    def _():
+        sent(fin, cast_send.at[0])
+
+    @pl.when(on_x | on_y)
+    def _():
+        sent(fin.at[:nchunks // 2], cast_send.at[0])
+
+    for d in range(nz - 1):
+        @pl.when(goes_up(d))
+        def _():
+            sent(wall.at[:wrows, :], up_send.at[d])
+
+        @pl.when(goes_down(d))
+        def _():
+            sent(wall.at[:wrows, :], down_send.at[d])
+
+    sent(wall.at[:nz * wrows, :], pair_send.at[0])
+
+    @pl.when(side_x | side_y)
+    def _():
+        sent(wall.at[:wrows // 2, :], side_send.at[0])
+
+    pltpu.make_async_copy(gq4, gq_out, gq_store.at[0]).wait()
+    pltpu.make_async_copy(gv8, gv_out, gv_store.at[0]).wait()
     pltpu.make_async_copy(gt, gt_out, gt_store.at[0]).wait()
+    gw_copy.wait()
 
 
 def whole(tokens, weight, queries, values, cotan, decay, nsp, ndp, heads):
@@ -685,7 +818,7 @@
             jax.ShapeDtypeStruct((rows, width), BF16),
             jax.ShapeDtypeStruct(queries.shape, BF16),
             jax.ShapeDtypeStruct(values.shape, BF16),
-            jax.ShapeDtypeStruct((wrows, width), BF16),
+            jax.ShapeDtypeStruct((nchunks, wrows, COLS), BF16),
         ],
         scratch_shapes=[
             buffer(rows, nsp * cwidth),
@@ -707,6 +840,7 @@
             buffer(*queries.shape),
             buffer(*values.shape),
             buffer(rows, width),
+            wide(width // TILE, rows, TILE),
             wide(nchunks, wrows, COLS),
             buffer(nchunks, wrows, COLS),
             buffer(nchunks, wrows, COLS),
@@ -721,22 +855,52 @@
             wide(heads, 8, vw),
             wide(heads, kw, vw),
             dma((8,)),
-            dma((nsp * heads,)), dma((nsp * heads,)),
-            dma((6 * nchunks,)), dma((6 * nchunks,)),
-            dma((nz * heads,)), dma((nz * heads,)),
-            dma((nz * heads,)), dma((nz * heads,)),
-            dma((nz * heads,)), dma((nz * heads,)),
-            dma((nsp,)), dma((nsp,)),
-            dma((nchunks,)), dma((nchunks,)),
-            dma((nchunks,)), dma((2 * nchunks,)),
-            dma((2 * nchunks,)), dma((2 * nchunks,)),
-            dma((nblocks,)), dma((nblocks,)), dma((nchunks,)), dma((1,)),
+            dma((1,)), dma(((nsp - 1) * heads,)),
+            dma((1,)), dma((2 * nchunks,)),
+            dma((nz - 1,)), dma(((nz - 1) * heads,)),
+            dma((nz - 1,)), dma(((nz - 1) * heads,)),
+            dma((1,)), dma((nz,)),
+            dma((1,)), dma((1,)),
+            dma((1,)), dma((1,)),
+            dma((1,)), dma((nchunks,)),
+            dma((1,)), dma((2 * nchunks,)),
+            dma((1,)), dma((nchunks + 1,)),
+            dma((1,)), dma((1,)), dma((1,)), dma((1,)),
         ],
         compiler_params=pltpu.CompilerParams(
             has_side_effects=True, vmem_limit_bytes=VMEM_LIMIT, collective_id=0
         ),
         name="whole",
     )(decay, tokens, weight, queries, values, cotan, jnp.asarray(cosine), jnp.asarray(sine))
+
+
+def finish_kernel(gt, gq, gv, gw, gt_out, gq_out, gv_out, gw_out):
+    gt_out[...] = gt[...]
+    gq_out[...] = gq[...]
+    gv_out[...] = gv[...]
+    for j in range(gw.shape[0]):
+        gw_out[:, j * COLS:(j + 1) * COLS] = gw[j].astype(F32)
+
+
+STEPS = 4
+
+
+def finish(gt, gq, gv, gw):
+    def flat(array):
+        return pl.BlockSpec((array.shape[0] // STEPS, array.shape[1]), lambda i: (i, 0))
+
+    chunks, wrows, cols = gw.shape
+    shapes = [(gt.shape, BF16), (gq.shape, BF16), (gv.shape, BF16), ((wrows, chunks * cols), F32)]
+    out_shape = [jax.ShapeDtypeStruct(*shape) for shape in shapes]
+    return pl.pallas_call(
+        finish_kernel,
+        grid=(STEPS,),
+        in_specs=[flat(gt), flat(gq), flat(gv)]
+        + [pl.BlockSpec((chunks, wrows // STEPS, cols), lambda i: (0, i, 0))],
+        out_specs=[flat(shape) for shape in out_shape],
+        out_shape=out_shape,
+        name="finish",
+    )(gt, gq, gv, gw)
 
 
 def gather_general(tokens, weight, cotan):
@@ -774,8 +938,10 @@
             tokens[0], key_weight, queries.reshape(-1, kw), flat.reshape(-1, LANES),
             cotangent[0], log_decay, nsp, ndp, heads,
         )
+        grad_tokens, grad_query, grad_value, weight_grad = finish(
+            grad_tokens, grad_query, grad_value, weight_grad
+        )
         grad_value = grad_value.reshape(seq_len, parts, heads, LANES).transpose(0, 2, 1, 3)
-        weight_grad = weight_grad.astype(F32)
     else:
         all_tokens, weight, cotan = gather_general(tokens[0], key_weight, cotangent[0])
         keys = dot_nt(all_tokens, weight).astype(BF16)

time: 131 us -> 116 us (0.89)
  the two profiles are of different devices: /device:TPU:3 before, /device:TPU:1 now
where the time goes in v2:
time: 116 us
  Pallas kernels  115 us (99%)
    pallas_call x1, Pallas kernels, whole(): pl.pallas_call(functools.partial(whole_kernel, nsp, nz, heads), in_specs=...  110 us
    pallas_call x1, Pallas kernels, finish(): pl.pallas_call(finish_kernel, grid=(STEPS,), in_specs=[flat(gt), flat(gq)...  5.48 us

profile of v2, /device:TPU:1, one launch (start us, length us, event | category | flops | bytes accessed | tf_op | source)
XLA Modules:
  0.0 115.8 jit_solution(14762247639549066154)
XLA Ops:
  0.6 109.7 %whole.1 = (bf16[256,2048]{1,0:T(8,128)(2,1)}, bf16[4096,128]{1,0:T(8,128)(2,1)}, bf16[8192,128]{1,0:T(8,128)(2,1)}, bf16[8,256,256]{2,1,0:T(8,128)(2,1)}) custom-call(f32[16]{0:T(128)} %decay_ref.1, bf16[256,2048]{1,0:T(8,128)(2,1)} %bitcast.17, bf16[256,2048]{1,0:T(8,128)(2,1)} %w_in.1, bf16[4096,128]{1,0:T(8,128)(2,1)} %bitcast.18, ...), custom_call_target="tpu_custom_call" | custom-call | tf_op jit(solution)/shard_map/whole/pallas_call | solution.py:813
  110.3 5.5 %finish.1 = (bf16[256,2048]{1,0:T(8,128)(2,1)}, bf16[4096,128]{1,0:T(8,128)(2,1)}, bf16[8192,128]{1,0:T(8,128)(2,1)}, f32[256,2048]{1,0:T(8,128)}) custom-call(bf16[256,2048]{1,0:T(8,128)(2,1)} %get-tuple-element.12.gt, bf16[4096,128]{1,0:T(8,128)(2,1)} %get-tuple-element.13.gq, bf16[8192,128]{1,0:T(8,128)(2,1)} %get-tuple-element.14.gv, ...), custom_call_target="tpu_custom_call" | custom-call | tf_op jit(solution)/shard_map/finish/pallas_call | solution.py:895

commit v3 on v2

--- a/solution.py
+++ b/solution.py
@@ -162,7 +162,7 @@
 TILE = 256
 LANES = 128
 COLS = 256
-HOP = 1
+HOP = 2
 
 
 def whole_kernel(
@@ -174,7 +174,7 @@
     within, rising, falling, carry, entering,
     load, cot_send, cot_recv, tok_send, tok_recv,
     up_send, up_recv, down_send, down_recv, pair_send, pair_recv, side_send, side_recv,
-    gk_send, gk_recv, half_send, half_recv, line_send, line_recv,
+    gk_sent, gk_recv, half_send, half_recv, line_send, line_recv,
     cast_send, cast_recv, gq_store, gv_store, gw_store, gt_store,
 ):
     s = lax.axis_index("sp")
@@ -483,13 +483,15 @@
 
     lax.fori_loop(0, heads, key_head, 0)
 
-    def gk_copy(j, source):
-        peer = (s + j) % nsp
-        to = gkall.at[:, pl.ds(pl.multiple_of(source * feats, feats), feats)]
-        return remote(
-            gk.at[pl.ds(pl.multiple_of(peer * rows, rows), rows), :], to,
-            gk_send.at[0], gk_recv.at[0], {"sp": peer},
-        )
+    def gk_send_head(h):
+        for j in range(1, nsp):
+            peer = (s + j) % nsp
+            source = gk.at[
+                pl.ds(pl.multiple_of(peer * rows, rows), rows),
+                pl.ds(pl.multiple_of(h * kw, kw), kw),
+            ]
+            to = gkall.at[:, pl.ds(pl.multiple_of(s * feats + h * kw, kw), kw)]
+            remote(source, to, gk_sent.at[0], gk_recv.at[0], {"sp": peer}).start()
 
     def half_copy(j):
         return remote(pwo.at[j], rp.at[j], half_send.at[0], half_recv.at[j], partner)
@@ -504,6 +506,24 @@
         ref = fin.at[j, pl.ds(h * (wrows // 2), wrows // 2), :]
         sem = cast_recv.at[nchunks if last_leg else j]
         return remote(ref, ref, cast_send.at[0], sem, {"sp": target})
+
+    def cast_side(j):
+        @pl.when(on_x)
+        def _():
+            received(fin.at[j, :wrows // 2, :], cast_recv.at[j])
+            cast_copy(j, 0, yn).start()
+
+        @pl.when(on_y)
+        def _():
+            received(fin.at[j, wrows // 2:, :], cast_recv.at[j])
+            cast_copy(j, 1, xn).start()
+
+    def cast_across(j):
+        @pl.when(on_d)
+        def _():
+            received(fin.at[j], cast_recv.at[j])
+            cast_copy(j, 0, xn, True).start()
+            cast_copy(j, 1, yn, True).start()
 
     def gradient_columns(j):
         token_wait(j, 4, 1)
@@ -624,6 +644,11 @@
             total = total + block_product((tardy + j) % nz, at)
         gtf[i] = total
 
+    def complete(i):
+        at = pl.ds(pl.multiple_of(i * TILE, TILE), TILE)
+        gt[:, at] = (gtf[i] + block_product(tardy, at)).astype(BF16)
+        gt_copy(i).start()
+
     last = nchunks + 1 + (nz + 1) * HOP
 
     def turn(t, _):
@@ -638,11 +663,6 @@
             for i in range(4):
                 token_send(t + 2, i).start()
 
-        @pl.when(t == nchunks - 1)
-        def _():
-            for j in range(1, nsp):
-                gk_copy(j, s).start()
-
         @pl.when((t >= 1) & (t <= nchunks))
         def _():
             gradient_columns(t - 1)
@@ -655,51 +675,61 @@
 
         jx = t - 2 - (far + 1) * HOP
 
-        @pl.when(on_x & (jx >= 0) & (jx < nchunks))
-        def _():
-            received(fin.at[jx, :wrows // 2, :], cast_recv.at[jx])
-            cast_copy(jx, 0, yn).start()
-
-        @pl.when(on_y & (jx >= 0) & (jx < nchunks))
-        def _():
-            received(fin.at[jx, wrows // 2:, :], cast_recv.at[jx])
-            cast_copy(jx, 1, xn).start()
+        @pl.when((jx >= 0) & (jx < nchunks))
+        def _():
+            cast_side(jx)
 
         jd = t - 2 - (far + 2) * HOP
 
-        @pl.when(on_d & (jd >= 0) & (jd < nchunks))
-        def _():
-            received(fin.at[jd], cast_recv.at[jd])
-            cast_copy(jd, 0, xn, True).start()
-            cast_copy(jd, 1, yn, True).start()
-
-        @pl.when(t < pieces)
-        def _():
-            relay_inward(t)
-
-        p = t - 2
-
-        @pl.when((p >= 0) & (p < pieces) & jnp.logical_not(opposite))
-        def _():
-            relay_second(p)
-
-        @pl.when((p >= 1) & (p <= pieces))
-        def _():
-            take_inward(p - 1)
-
-        p = t - jnp.where(opposite, pieces, nchunks + 1)
-
-        @pl.when((p >= 0) & (p < pieces))
-        def _():
-            relay_third(p)
-
-        p = t - nchunks - 1
-
-        @pl.when(opposite & (p >= 0) & (p < pieces))
-        def _():
-            relay_second(p)
-
-        @pl.when(t == pieces + 2)
+        @pl.when((jd >= 0) & (jd < nchunks))
+        def _():
+            cast_across(jd)
+
+        @pl.when((t >= nchunks - 1) & (t < nchunks - 1 + heads))
+        def _():
+            gk_send_head(t - (nchunks - 1))
+
+        beat, on_beat = t // unit, t % unit == 0
+
+        for p in range(pieces):
+            when = jnp.where(patient, sum_step, sends[p]) if p == pieces - 1 else sends[p]
+
+            @pl.when(t == when)
+            def _():
+                relay_inward(p)
+
+            when = jnp.where(awaits, sum_step + 4, takes[p]) if p == pieces - 1 else takes[p]
+
+            @pl.when(t == when)
+            def _():
+                take_inward(p)
+
+        after = t - nchunks - 1
+        slot = after // 2
+        on_slot = (after >= 0) & (after < 2 * pieces) & (after % 2 == 0)
+        ahead = jnp.where(opposite, beat - pieces, beat - 2)
+
+        @pl.when(on_beat & (ahead >= 0) & (ahead < pieces))
+        def _():
+            @pl.when(opposite)
+            def _():
+                relay_third(ahead)
+
+            @pl.when(jnp.logical_not(opposite))
+            def _():
+                relay_second(ahead)
+
+        @pl.when(on_slot)
+        def _():
+            @pl.when(opposite)
+            def _():
+                relay_second(slot)
+
+            @pl.when(jnp.logical_not(opposite))
+            def _():
+                relay_third(slot)
+
+        @pl.when(t == unit * (pieces + 2))
         def _():
             relay_rest()
 
@@ -707,12 +737,10 @@
         def _():
             make_keys()
 
-        n = (t - nchunks - 1) * 2
-
-        @pl.when((n >= 0) & (n < nblocks))
-        def _():
-            query_block(n)
-            query_block(n + 1)
+        @pl.when((after >= 0) & (after < nblocks // 2))
+        def _():
+            query_block(2 * after)
+            query_block(2 * after + 1)
 
         i = t - tile_step
 
@@ -725,25 +753,34 @@
             token_gradient(2 * i)
             token_gradient(2 * i + 1)
 
+        @pl.when(t == last - 3)
+        def _():
+            take_side()
+
+        @pl.when(t == last - 2)
+        def _():
+            @pl.when(tardy != s)
+            def _():
+                pair_wait(tardy)
+
+        @pl.when((t == last - 2) | (t == last - 1))
+        def _():
+            first = (t - (last - 2)) * (ntiles // 2)
+            for i in range(ntiles // 2):
+                complete(first + i)
+
         return 0
 
     ntiles = width // TILE
-    tile_step = nchunks + HOP + 2
+    tile_step = nchunks + 5
+    unit = nchunks // 8
+    sends = [unit * (p * (p + 3) // 4) for p in range(pieces)]
+    takes = [unit * (2 * p + 3) for p in range(pieces)]
+    sum_step = nchunks + 1 + HOP
+    outer = (s == 0) | (s == nz - 1)
+    patient = outer & (behind == 1) & jnp.logical_not(owner)
+    awaits = outer & (behind == 2) & jnp.logical_not(owner)
     lax.fori_loop(0, last + 1, turn, 0)
-    take_side()
-
-    @pl.when(tardy != s)
-    def _():
-        pair_wait(tardy)
-
-    def complete(i, _):
-        at = pl.ds(pl.multiple_of(i * TILE, TILE), TILE)
-        gt[:, at] = (gtf[i] + block_product(tardy, at)).astype(BF16)
-        gt_copy(i).start()
-        return 0
-
-    lax.fori_loop(0, ntiles, complete, 0)
-
     @pl.when(on_x | on_y)
     def _():
         received(fin.at[:nchunks // 2], cast_recv.at[nchunks])
@@ -753,7 +790,7 @@
 
     sent(cotv.at[:, :(nsp - 1) * cwidth], cot_send.at[0])
     sent(tall.at[:6 * hrows, :], tok_send.at[0])
-    sent(gk.at[:(nsp - 1) * rows, :], gk_send.at[0])
+    sent(gk.at[:(nsp - 1) * rows, :], gk_sent.at[0])
     sent(pwo, half_send.at[0])
 
     @pl.when(jnp.logical_not(owner))
@@ -874,31 +911,48 @@
     )(decay, tokens, weight, queries, values, cotan, jnp.asarray(cosine), jnp.asarray(sine))
 
 
-def finish_kernel(gt, gq, gv, gw, gt_out, gq_out, gv_out, gw_out):
-    gt_out[...] = gt[...]
-    gq_out[...] = gq[...]
-    gv_out[...] = gv[...]
-    for j in range(gw.shape[0]):
-        gw_out[:, j * COLS:(j + 1) * COLS] = gw[j].astype(F32)
-
-
-STEPS = 4
+def finish_kernel(gt, gq, gv, gw, gt_out, gq_out, gv_out, gw_out, bt, bq, bv, bw, bf, get, put):
+    chunks, wrows = gw.shape[:2]
+    reads, writes = [], []
+    for source, held, target, count in (
+        (gw, bw, None, 2), (gv, bv, gv_out, 4), (gq, bq, gq_out, 2), (gt, bt, gt_out, 2)
+    ):
+        axis = source.shape[0] // count
+        for i in range(count):
+            at = pl.ds(i * axis, axis)
+            n = len(reads)
+            reads.append(pltpu.make_async_copy(source.at[at], held.at[at], get.at[n]))
+            if target is not None:
+                writes.append(pltpu.make_async_copy(held.at[at], target.at[at], put.at[n]))
+            else:
+                into = pl.ds(i * axis * COLS, axis * COLS)
+                writes.append(pltpu.make_async_copy(bf.at[:, into], gw_out.at[:, into], put.at[n]))
+    for read in reads:
+        read.start()
+    for n, (read, write) in enumerate(zip(reads, writes)):
+        read.wait()
+        if n < 2:
+            for j in range(n * chunks // 2, (n + 1) * chunks // 2):
+                bf[:, j * COLS:(j + 1) * COLS] = bw[j].astype(F32)
+        write.start()
+    for write in writes:
+        write.wait()
 
 
 def finish(gt, gq, gv, gw):
-    def flat(array):
-        return pl.BlockSpec((array.shape[0] // STEPS, array.shape[1]), lambda i: (i, 0))
-
     chunks, wrows, cols = gw.shape
-    shapes = [(gt.shape, BF16), (gq.shape, BF16), (gv.shape, BF16), ((wrows, chunks * cols), F32)]
-    out_shape = [jax.ShapeDtypeStruct(*shape) for shape in shapes]
+    arrays = [gt, gq, gv, gw]
+    total = (wrows, chunks * cols)
+    anywhere = pl.BlockSpec(memory_space=pl.ANY)
     return pl.pallas_call(
         finish_kernel,
-        grid=(STEPS,),
-        in_specs=[flat(gt), flat(gq), flat(gv)]
-        + [pl.BlockSpec((chunks, wrows // STEPS, cols), lambda i: (0, i, 0))],
-        out_specs=[flat(shape) for shape in out_shape],
-        out_shape=out_shape,
+        in_specs=[anywhere] * 4,
+        out_specs=[anywhere] * 4,
+        out_shape=[jax.ShapeDtypeStruct(array.shape, BF16) for array in arrays[:3]]
+        + [jax.ShapeDtypeStruct(total, F32)],
+        scratch_shapes=[pltpu.VMEM(array.shape, BF16) for array in arrays]
+        + [pltpu.VMEM(total, F32), pltpu.SemaphoreType.DMA((10,)), pltpu.SemaphoreType.DMA((10,))],
+        compiler_params=pltpu.CompilerParams(vmem_limit_bytes=VMEM_LIMIT),
         name="finish",
     )(gt, gq, gv, gw)
 

time: 116 us -> 103 us (0.89)
  Pallas kernels: 115 us -> 102 us
    pallas_call x1, Pallas kernels: 110 us -> 97.7 us  [whole(): pl.pallas_call(functools.partial(whole_kernel, nsp, nz, heads), in_specs=...]
where the time goes in v3:
time: 103 us
  Pallas kernels  102 us (99%)
    pallas_call x1, Pallas kernels, whole(): pl.pallas_call(functools.partial(whole_kernel, nsp, nz, heads), in_specs=...  97.7 us
    pallas_call x1, Pallas kernels, finish(): pl.pallas_call(finish_kernel, in_specs=[anywhere] * 4, out_specs=[anywher...  4.55 us

profile of v3, /device:TPU:1, one launch (start us, length us, event | category | flops | bytes accessed | tf_op | source)
XLA Modules:
  0.0 102.9 jit_solution(8713026565397807825)
XLA Ops:
  0.6 97.7 %whole.1 = (bf16[256,2048]{1,0:T(8,128)(2,1)}, bf16[4096,128]{1,0:T(8,128)(2,1)}, bf16[8192,128]{1,0:T(8,128)(2,1)}, bf16[8,256,256]{2,1,0:T(8,128)(2,1)}) custom-call(f32[16]{0:T(128)} %decay_ref.1, bf16[256,2048]{1,0:T(8,128)(2,1)} %bitcast.17, bf16[256,2048]{1,0:T(8,128)(2,1)} %w_in.1, bf16[4096,128]{1,0:T(8,128)(2,1)} %bitcast.18, ...), custom_call_target="tpu_custom_call" | custom-call | tf_op jit(solution)/shard_map/whole/pallas_call | solution.py:850
  98.4 4.5 %finish.1 = (bf16[256,2048]{1,0:T(8,128)(2,1)}, bf16[4096,128]{1,0:T(8,128)(2,1)}, bf16[8192,128]{1,0:T(8,128)(2,1)}, f32[256,2048]{1,0:T(8,128)}) custom-call(bf16[256,2048]{1,0:T(8,128)(2,1)} %get-tuple-element.12.gt, bf16[4096,128]{1,0:T(8,128)(2,1)} %get-tuple-element.13.gq, bf16[8192,128]{1,0:T(8,128)(2,1)} %get-tuple-element.14.gv, ...), custom_call_target="tpu_custom_call" | custom-call | tf_op jit(solution)/shard_map/finish/pallas_call | solution.py:947

commit v4 on v3

--- a/solution.py
+++ b/solution.py
@@ -163,6 +163,7 @@
 LANES = 128
 COLS = 256
 HOP = 2
+CAST = 3
 
 
 def whole_kernel(
@@ -291,8 +292,10 @@
     def goes_down(d):
         return (z + d < nz) & (z > 0 if d < nz - 2 else (z > 0) & (s != 0))
 
-    def side_copy(p, target):
-        ref = piece(nz - 1 - z, core, p)
+    def side_copy(p, part, target):
+        zb = nz - 1 - z
+        start = pl.multiple_of((zb * CORES + core) * wrows + p * prow + part * (prow // 2), prow // 2)
+        ref = wall.at[pl.ds(start, prow // 2), :]
         return remote(ref, ref, side_send.at[0], side_recv.at[0], {"sp": target})
 
     def rise_of(d, p):
@@ -372,13 +375,13 @@
         def _():
             fall_of(3, p)
 
-        @pl.when(side_x & (p < pieces // 2))
-        def _():
-            side_copy(p, xn).start()
-
-        @pl.when(side_y & (p >= pieces // 2))
-        def _():
-            side_copy(p, yn).start()
+        @pl.when(side_x)
+        def _():
+            side_copy(p, 0, xn).start()
+
+        @pl.when(side_y)
+        def _():
+            side_copy(p, 1, yn).start()
 
     def prompt(p, yields):
         return jnp.logical_not(yields & (p > 0))
@@ -649,7 +652,7 @@
         gt[:, at] = (gtf[i] + block_product(tardy, at)).astype(BF16)
         gt_copy(i).start()
 
-    last = nchunks + 1 + (nz + 1) * HOP
+    last = nchunks + 1 + (nz - 1) * HOP + 2 * CAST
 
     def turn(t, _):
         @pl.when(t < nchunks)
@@ -673,21 +676,21 @@
         def _():
             sum_line(j)
 
-        jx = t - 2 - (far + 1) * HOP
+        jx = t - 2 - far * HOP - CAST
 
         @pl.when((jx >= 0) & (jx < nchunks))
         def _():
             cast_side(jx)
 
-        jd = t - 2 - (far + 2) * HOP
+        jd = t - 2 - far * HOP - 2 * CAST
 
         @pl.when((jd >= 0) & (jd < nchunks))
         def _():
             cast_across(jd)
 
-        @pl.when((t >= nchunks - 1) & (t < nchunks - 1 + heads))
-        def _():
-            gk_send_head(t - (nchunks - 1))
+        @pl.when((t >= nchunks) & (t < nchunks + heads))
+        def _():
+            gk_send_head(t - nchunks)
 
         beat, on_beat = t // unit, t % unit == 0
 
@@ -733,14 +736,14 @@
         def _():
             relay_rest()
 
-        @pl.when(t == nchunks)
+        @pl.when(after == 0)
         def _():
             make_keys()
 
-        @pl.when((after >= 0) & (after < nblocks // 2))
-        def _():
-            query_block(2 * after)
-            query_block(2 * after + 1)
+        @pl.when((after >= 1) & (after <= nblocks // 2))
+        def _():
+            query_block(2 * after - 2)
+            query_block(2 * after - 1)
 
         i = t - tile_step
 
@@ -774,7 +777,7 @@
     ntiles = width // TILE
     tile_step = nchunks + 5
     unit = nchunks // 8
-    sends = [unit * (p * (p + 3) // 4) for p in range(pieces)]
+    sends = [unit * p for p in range(pieces)]
     takes = [unit * (2 * p + 3) for p in range(pieces)]
     sum_step = nchunks + 1 + HOP
     outer = (s == 0) | (s == nz - 1)

time: 103 us -> 101 us (0.981)
  Pallas kernels: 102 us -> 99.7 us
    pallas_call x1, Pallas kernels: 97.7 us -> 95.2 us  [whole(): pl.pallas_call(functools.partial(whole_kernel, nsp, nz, heads), in_specs=...]
where the time goes in v4:
time: 101 us; the launch traced here: 100 us
  Pallas kernels  99.7 us (99%)
    pallas_call x1, Pallas kernels, whole(): pl.pallas_call(functools.partial(whole_kernel, nsp, nz, heads), in_specs=...  95.2 us
    pallas_call x1, Pallas kernels, finish(): pl.pallas_call(finish_kernel, in_specs=[anywhere] * 4, out_specs=[anywher...  4.55 us

profile of v4, /device:TPU:1, one launch (start us, length us, event | category | flops | bytes accessed | tf_op | source)
XLA Modules:
  0.0 100.4 jit_solution(798383095497112151)
XLA Ops:
  0.6 95.2 %whole.1 = (bf16[256,2048]{1,0:T(8,128)(2,1)}, bf16[4096,128]{1,0:T(8,128)(2,1)}, bf16[8192,128]{1,0:T(8,128)(2,1)}, bf16[8,256,256]{2,1,0:T(8,128)(2,1)}) custom-call(f32[16]{0:T(128)} %decay_ref.1, bf16[256,2048]{1,0:T(8,128)(2,1)} %bitcast.17, bf16[256,2048]{1,0:T(8,128)(2,1)} %w_in.1, bf16[4096,128]{1,0:T(8,128)(2,1)} %bitcast.18, ...), custom_call_target="tpu_custom_call" | custom-call | tf_op jit(solution)/shard_map/whole/pallas_call | solution.py:853
  95.8 4.5 %finish.1 = (bf16[256,2048]{1,0:T(8,128)(2,1)}, bf16[4096,128]{1,0:T(8,128)(2,1)}, bf16[8192,128]{1,0:T(8,128)(2,1)}, f32[256,2048]{1,0:T(8,128)}) custom-call(bf16[256,2048]{1,0:T(8,128)(2,1)} %get-tuple-element.12.gt, bf16[4096,128]{1,0:T(8,128)(2,1)} %get-tuple-element.13.gq, bf16[8192,128]{1,0:T(8,128)(2,1)} %get-tuple-element.14.gv, ...), custom_call_target="tpu_custom_call" | custom-call | tf_op jit(solution)/shard_map/finish/pallas_call | solution.py:950

commit v5 on v4

--- a/solution.py
+++ b/solution.py
@@ -778,7 +778,7 @@
     tile_step = nchunks + 5
     unit = nchunks // 8
     sends = [unit * p for p in range(pieces)]
-    takes = [unit * (2 * p + 3) for p in range(pieces)]
+    takes = [unit * (3 + p + p // 2) for p in range(pieces)]
     sum_step = nchunks + 1 + HOP
     outer = (s == 0) | (s == nz - 1)
     patient = outer & (behind == 1) & jnp.logical_not(owner)

time: 101 us -> 101 us (level)
  no operation moved by 1% of the time
where the time goes in v5:
time: 101 us; the launch traced here: 100 us
  Pallas kernels  99.7 us (99%)
    pallas_call x1, Pallas kernels, whole(): pl.pallas_call(functools.partial(whole_kernel, nsp, nz, heads), in_specs=...  95.2 us
    pallas_call x1, Pallas kernels, finish(): pl.pallas_call(finish_kernel, in_specs=[anywhere] * 4, out_specs=[anywher...  4.55 us

profile of v5, /device:TPU:1, one launch (start us, length us, event | category | flops | bytes accessed | tf_op | source)
XLA Modules:
  0.0 100.4 jit_solution(16314730020685376414)
XLA Ops:
  0.6 95.2 %whole.1 = (bf16[256,2048]{1,0:T(8,128)(2,1)}, bf16[4096,128]{1,0:T(8,128)(2,1)}, bf16[8192,128]{1,0:T(8,128)(2,1)}, bf16[8,256,256]{2,1,0:T(8,128)(2,1)}) custom-call(f32[16]{0:T(128)} %decay_ref.1, bf16[256,2048]{1,0:T(8,128)(2,1)} %bitcast.17, bf16[256,2048]{1,0:T(8,128)(2,1)} %w_in.1, bf16[4096,128]{1,0:T(8,128)(2,1)} %bitcast.18, ...), custom_call_target="tpu_custom_call" | custom-call | tf_op jit(solution)/shard_map/whole/pallas_call | solution.py:853
  95.8 4.5 %finish.1 = (bf16[256,2048]{1,0:T(8,128)(2,1)}, bf16[4096,128]{1,0:T(8,128)(2,1)}, bf16[8192,128]{1,0:T(8,128)(2,1)}, f32[256,2048]{1,0:T(8,128)}) custom-call(bf16[256,2048]{1,0:T(8,128)(2,1)} %get-tuple-element.12.gt, bf16[4096,128]{1,0:T(8,128)(2,1)} %get-tuple-element.13.gq, bf16[8192,128]{1,0:T(8,128)(2,1)} %get-tuple-element.14.gv, ...), custom_call_target="tpu_custom_call" | custom-call | tf_op jit(solution)/shard_map/finish/pallas_call | solution.py:950
